TPU v7x, 32 devices: a whole 2x2x4 slice. The times are simulated.
32 devices in a mesh: ep: 16 (over z, x, core), tp: 2 (over y).
Axes of the slice: x: 2, y: 2, z: 4, core: 2. Of those that a mesh axis runs over, the one named last changes fastest.
Arguments:
- tokens: bfloat16 [2048, 2048], P('ep'), may hold values from -6 to 6
- cotangent: bfloat16 [2048, 2048], P('ep'), may hold values from -1.796875 to 1.796875
- group_weight: float32 [2048], P('ep'), may hold values from 0.2 to 1
- expert_weight: float32 [2048, 2], P('ep'), may hold values from 0.1 to 0.9
- group_choice: int32 [2048], P('ep'), may hold values from 0 to 3, as said below
- local_choice: int32 [2048, 2], P('ep'), may hold values from 0 to 3, as said below
- w_gate: bfloat16 [16, 2048, 512], P('ep', None, 'tp'), may hold values from -0.125 to 0.125
- w_up: bfloat16 [16, 2048, 512], P('ep', None, 'tp'), may hold values from -0.125 to 0.125
- w_down: bfloat16 [16, 512, 2048], P('ep', 'tp'), may hold values from -0.25 to 0.25
Outputs:
- token_grad: float32 [2048, 2048], P('ep', 'tp')
- group_weight_grad: float32 [2048], P('ep')
- expert_weight_grad: float32 [2048, 2], P('ep')
- w_gate_grad: float32 [16, 2048, 512], P('ep', None, 'tp')
- w_up_grad: float32 [16, 2048, 512], P('ep', None, 'tp')
- w_down_grad: float32 [16, 512, 2048], P('ep', 'tp')
Inputs may be any that keep to these rules, and one draw needn't show every extreme that they name: Among the 128 tokens of each device (aligned blocks of tokens), no expert 4 * group_choice + local_choice is named by more than 24 slots, and some expert is named by exactly 24 slots of every device. `local_choice`: the 2 local choices of a token differ.
All inputs are finite; a program needn't handle non-finite values.
Results may differ from a plain program's by a relative error of at most 0.006.
Values may be sent and summed in bfloat16 or wider, within the bound.
A program may use at most 64 MiB of HBM per device.

v0:
```python
import functools

import jax
import jax.numpy as jnp
from jax import lax
from jax.experimental import pallas as pl
from jax.experimental.pallas import tpu as pltpu
from jax.sharding import Mesh, PartitionSpec as P

EPG = 4
LANES = 128

MESH = pl.DeviceIdType.MESH


def place():
    g, e, y = lax.axis_index("g"), lax.axis_index("e"), lax.axis_index("tp")
    x, c = e // 2, e % 2
    return g, e, y, x, c


def partner(g, d, groups, sign):
    if groups & (groups - 1):
        return lax.rem(g + sign * d + groups, groups)
    met, bit = g, 1
    while bit < groups:
        if d & bit:
            met = met + bit - 2 * bit * ((g // bit) % 2)
        bit *= 2
    return met


def greet(devices):
    barrier = pltpu.get_barrier_semaphore()
    for device in devices:
        pl.semaphore_signal(barrier, inc=1, device_id=device, device_id_type=MESH)
    pl.semaphore_wait(barrier, len(devices))


class Copies:
    def __init__(self, send_sem, recv_sem):
        self.send_sem, self.recv_sem, self.made = send_sem, recv_sem, []

    def start(self, src, dst, device):
        number = len(self.made)
        copy = pltpu.make_async_remote_copy(
            src_ref=src,
            dst_ref=dst,
            send_sem=self.send_sem.at[number],
            recv_sem=self.recv_sem.at[number],
            device_id=device,
            device_id_type=MESH,
        )
        copy.start()
        self.made.append(copy)
        return copy

    def finish(self):
        for copy in self.made:
            copy.wait_send()


def window(start, size, unit):
    return pl.ds(pl.multiple_of(start, unit), size)


def forward_count(groups, lanes):
    return (groups - 1) * 3 + groups * (3 * (lanes - 1) + 9)


def forward_kernel(groups, lanes, cap, piece, tok_in, cot_in, gate_in, tok, cot, gate, send, recv, loc):
    g, e, y, x, c = place()
    rows = groups * cap
    ex, ec, exc = (1 - x) * 2 + c, x * 2 + (1 - c), (1 - x) * 2 + (1 - c)
    others = [(g, e, lax.rem(y + r, lanes)) for r in range(1, lanes)]
    greet(
        [(lax.rem(g + d, groups), e, y) for d in range(1, groups)]
        + others
        + [(g, ex, y), (g, ec, y), (g, exc, y)]
    )
    copies = Copies(send, recv)
    cols = window(y * piece, piece, LANES)

    def block(ref, owner, source, columns=slice(None)):
        return ref.at[window(owner * rows + source * cap, cap, 16), columns]

    def inner(ref, group):
        return ref.at[window(group * cap, cap, 16), :]

    first = []
    pairs = ((tok_in, tok, cols), (cot_in, cot, cols), (gate_in, gate, slice(None)))
    for d in range(groups):
        target = partner(g, d, groups, -1)
        made = []
        for i, (src, dst, columns) in enumerate(pairs):
            if d == 0:
                copy = pltpu.make_async_copy(inner(src, g), block(dst, e, g, columns), loc.at[i])
                copy.start()
            else:
                copy = copies.start(inner(src, target), block(dst, e, g, columns), (target, e, y))
            made.append(copy)
        first.append(made)
    state = [dict() for _ in range(groups)]
    last = []

    def stage_a(d):
        source = partner(g, d, groups, 1)
        for copy in first[d]:
            if d == 0:
                copy.wait()
            else:
                copy.wait_recv()
        own_t, own_c = block(tok, e, source, cols), block(cot, e, source, cols)
        state[d]["tl"] = [copies.start(own_t, own_t, device) for device in others]
        state[d]["cx"] = copies.start(own_c, own_c, (g, ex, y))
        state[d]["cl"] = [copies.start(own_c, own_c, device) for device in others]
        own_g = block(gate, e, source)
        for peer in (ex, ec, exc):
            last.append(copies.start(own_g, own_g, (g, peer, y)))

    def stage_b(d):
        source = partner(g, d, groups, 1)
        for copy in state[d]["tl"]:
            copy.wait_recv()
        full = block(tok, e, source)
        state[d]["tx"] = copies.start(full, full, (g, ex, y))
        state[d]["cx"].wait_recv()
        part = block(cot, ex, source, cols)
        state[d]["cxl"] = [copies.start(part, part, device) for device in others]
        last.append(copies.start(full, full, (g, ec, y)))

    def stage_c(d):
        source = partner(g, d, groups, 1)
        for copy in state[d]["cl"]:
            copy.wait_recv()
        full = block(cot, e, source)
        last.append(copies.start(full, full, (g, ec, y)))
        state[d]["tx"].wait_recv()
        full = block(tok, ex, source)
        last.append(copies.start(full, full, (g, ec, y)))
        for copy in state[d]["cxl"]:
            copy.wait_recv()
        full = block(cot, ex, source)
        last.append(copies.start(full, full, (g, ec, y)))

    for step in range(groups + 2):
        if step < groups:
            stage_a(step)
        if 0 <= step - 1 < groups:
            stage_b(step - 1)
        if 0 <= step - 2 < groups:
            stage_c(step - 2)
    for copy in last:
        copy.wait_recv()
    copies.finish()


def forward(tok_in, cot_in, gate_in, groups, lanes, cap, piece):
    all_rows = EPG * groups * cap
    count = forward_count(groups, lanes)
    vmem = pl.BlockSpec(memory_space=pltpu.VMEM)
    return pl.pallas_call(
        functools.partial(forward_kernel, groups, lanes, cap, piece),
        out_shape=(
            jax.ShapeDtypeStruct((all_rows, lanes * piece), jnp.bfloat16),
            jax.ShapeDtypeStruct((all_rows, lanes * piece), jnp.bfloat16),
            jax.ShapeDtypeStruct((all_rows, LANES), jnp.bfloat16),
        ),
        in_specs=[vmem] * 3,
        out_specs=(vmem,) * 3,
        scratch_shapes=[
            pltpu.SemaphoreType.DMA((count,)),
            pltpu.SemaphoreType.DMA((count,)),
            pltpu.SemaphoreType.DMA((3,)),
        ],
        compiler_params=pltpu.CompilerParams(collective_id=0, has_side_effects=True),
        name="forward_exchange",
    )(tok_in, cot_in, gate_in)


def add(*parts):
    total = parts[0].astype(jnp.float32)
    for part in parts[1:]:
        total = total + part.astype(jnp.float32)
    return total.astype(jnp.bfloat16)


def return_kernel(
    groups, lanes, cap, wide0, wide1, part, out, rc, s1, rx0, s2a, rl0, rl1, s2b, rx1, done, send, recv
):
    g, e, y, x, c = place()
    rows = groups * cap
    ex, ec = (1 - x) * 2 + c, x * 2 + (1 - c)
    others = [(g, e, lax.rem(y + r, lanes)) for r in range(1, lanes)]
    greet(
        [(lax.rem(g + d, groups), e, y) for d in range(1, groups)]
        + others
        + [(g, ex, y), (g, ec, y)]
    )
    copies = Copies(send, recv)
    all0 = lanes * wide0
    head, tail = pl.ds(0, all0), pl.ds(all0, lanes * wide1)

    def at(index, source):
        return window(index * rows + source * cap, cap, 16)

    def lane0(lane):
        return window(lane * wide0, wide0, LANES)

    def lane1(lane):
        return window(all0 + lane * wide1, wide1, LANES)

    order = list(range(groups // 2, groups)) + list(range(1, groups // 2)) + [0]
    sources = [partner(g, d, groups, 1) for d in order]
    state = [dict() for _ in order]
    for i, s in enumerate(sources):
        state[i]["core"] = [
            copies.start(part.at[at(2 * k + 1 - c, s), :], rc.at[at(k, s), :], (g, ec, y))
            for k in range(2)
        ]

    def stage_a(i):
        s = sources[i]
        for k in range(2):
            state[i]["core"][k].wait_recv()
            for columns in (head, tail):
                s1[at(k, s), columns] = add(part[at(2 * k + c, s), columns], rc[at(k, s), columns])
        state[i]["x0"] = copies.start(s1.at[at(1 - x, s), head], rx0.at[at(0, s), :], (g, ex, y))
        state[i]["l1"] = [
            copies.start(
                s1.at[at(k, s), lane1(device[2])], rl1.at[at(2 * r + k, s), :], device
            )
            for r, device in enumerate(others)
            for k in range(2)
        ]

    def stage_b(i):
        s = sources[i]
        state[i]["x0"].wait_recv()
        s2a[at(0, s), :] = add(s1[at(x, s), head], rx0[at(0, s), :])
        state[i]["l0"] = [
            copies.start(s2a.at[at(0, s), lane0(device[2])], rl0.at[at(r, s), :], device)
            for r, device in enumerate(others)
        ]
        for copy in state[i]["l1"]:
            copy.wait_recv()
        for k in range(2):
            s2b[at(k, s), :] = add(
                s1[at(k, s), lane1(y)], *[rl1[at(2 * r + k, s), :] for r in range(lanes - 1)]
            )
        state[i]["x1"] = copies.start(s2b.at[at(1 - x, s), :], rx1.at[at(0, s), :], (g, ex, y))

    def stage_c(i):
        s = sources[i]
        target = out if order[i] == 0 else done
        for copy in state[i]["l0"]:
            copy.wait_recv()
        target[at(0, s), pl.ds(0, wide0)] = add(
            s2a[at(0, s), lane0(y)], *[rl0[at(r, s), :] for r in range(lanes - 1)]
        )
        state[i]["x1"].wait_recv()
        target[at(0, s), pl.ds(wide0, wide1)] = add(s2b[at(x, s), :], rx1[at(0, s), :])
        if order[i] != 0:
            state[i]["z"] = copies.start(done.at[at(0, s), :], out.at[at(0, g), :], (s, e, y))

    for step in range(groups + 2):
        if step < groups:
            stage_a(step)
        if 0 <= step - 1 < groups:
            stage_b(step - 1)
        if 0 <= step - 2 < groups:
            stage_c(step - 2)
    for i in range(groups):
        if order[i] != 0:
            state[i]["z"].wait_recv()
    copies.finish()


def give_back(part, groups, lanes, cap, wide0, wide1):
    rows = groups * cap
    count = (groups - 1) + groups * (4 + 3 * (lanes - 1))
    vmem = pl.BlockSpec(memory_space=pltpu.VMEM)
    wide = lanes * (wide0 + wide1)
    far = max(lanes - 1, 1)

    def buffer(height, width):
        return pltpu.VMEM((height, width), jnp.bfloat16)

    return pl.pallas_call(
        functools.partial(return_kernel, groups, lanes, cap, wide0, wide1),
        out_shape=jax.ShapeDtypeStruct((rows, wide0 + wide1), jnp.bfloat16),
        in_specs=[vmem],
        out_specs=vmem,
        scratch_shapes=[
            buffer(2 * rows, wide),
            buffer(2 * rows, wide),
            buffer(rows, lanes * wide0),
            buffer(rows, lanes * wide0),
            buffer(far * rows, wide0),
            buffer(far * 2 * rows, wide1),
            buffer(2 * rows, wide1),
            buffer(rows, wide1),
            buffer(rows, wide0 + wide1),
            pltpu.SemaphoreType.DMA((count,)),
            pltpu.SemaphoreType.DMA((count,)),
        ],
        compiler_params=pltpu.CompilerParams(collective_id=1, has_side_effects=True),
        name="return_exchange",
    )(part)


def shards(
    tokens, cotangent, group_weight, expert_weight, group_choice, local_choice, w_gate, w_up, w_down
):
    token_count, feature_count = tokens.shape
    pick_count = expert_weight.shape[1]
    group_count = lax.axis_size("g")
    lane_count = lax.axis_size("tp")
    expert_count = group_count * EPG
    capacity = pick_count * (3 * token_count // (2 * expert_count))
    group_cap = -(-(EPG * capacity // pick_count) // 16) * 16
    row_count = group_count * group_cap
    piece = feature_count // lane_count
    order = jnp.arange(token_count, dtype=jnp.int32)
    same = (group_choice[:, None] == group_choice[None, :]) & (order[:, None] > order[None, :])
    dest = group_choice * group_cap + jnp.sum(same.astype(jnp.int32), axis=1)
    pick = (jnp.arange(row_count, dtype=jnp.int32)[:, None] == dest[None, :]).astype(jnp.bfloat16)
    gate = (group_weight[:, None] * expert_weight).astype(jnp.bfloat16)
    named = local_choice[:, :, None] == jnp.arange(LANES, dtype=jnp.int32)
    gate_cols = jnp.sum(jnp.where(named, gate[:, :, None], 0), axis=1).astype(jnp.bfloat16)
    lane = lax.axis_index("tp")
    token_cols = lax.dynamic_slice_in_dim(tokens, lane * piece, piece, 1)
    cot_cols = lax.dynamic_slice_in_dim(cotangent, lane * piece, piece, 1)
    payload = jnp.concatenate([token_cols, cot_cols, gate_cols], axis=1)
    rows = jnp.dot(pick, payload, preferred_element_type=jnp.float32).astype(jnp.bfloat16)
    arrived, cot_rows, gate_block = forward(
        rows[:, :piece],
        rows[:, piece : 2 * piece],
        rows[:, 2 * piece :],
        group_count,
        lane_count,
        group_cap,
        piece,
    )
    own = jnp.arange(LANES, dtype=jnp.int32) == lax.axis_index("e")
    gate_block = gate_block.astype(jnp.float32)
    gate_float = jnp.sum(jnp.where(own, gate_block, 0.0), axis=1, keepdims=True)
    first, second, third = w_gate[0], w_up[0], w_down[0]
    contract_cols = (((1,), (1,)), ((), ()))
    contract_rows = (((0,), (0,)), ((), ()))
    pre_gate = jnp.dot(arrived, first, preferred_element_type=jnp.float32)
    pre_up = jnp.dot(arrived, second, preferred_element_type=jnp.float32)
    back = lax.dot_general(cot_rows, third, contract_cols, preferred_element_type=jnp.float32)
    sigma = jax.nn.sigmoid(pre_gate)
    swish = pre_gate * sigma
    hidden = swish * pre_up
    gate_part = jnp.sum(hidden * back, axis=1, keepdims=True)
    scaled = gate_float * back
    grad_gate = (scaled * pre_up * sigma * (1.0 + pre_gate * (1.0 - sigma))).astype(jnp.bfloat16)
    grad_up = (scaled * swish).astype(jnp.bfloat16)
    weighted = (gate_float * hidden).astype(jnp.bfloat16)
    partial_rows = lax.dot_general(
        grad_gate, first, contract_cols, preferred_element_type=jnp.float32
    ) + lax.dot_general(grad_up, second, contract_cols, preferred_element_type=jnp.float32)
    partial_rows = partial_rows.astype(jnp.bfloat16)
    gate_out = jnp.where(own, gate_part, 0.0).astype(jnp.bfloat16)
    wide1 = (piece + LANES) // (2 * LANES) * LANES
    wide0 = piece + LANES - wide1
    back_rows = jnp.concatenate(
        [partial_rows[:, y * piece : y * piece + wide0] for y in range(lane_count)]
        + [
            column
            for y in range(lane_count)
            for column in (partial_rows[:, y * piece + wide0 : (y + 1) * piece], gate_out)
        ],
        axis=1,
    )
    returned = give_back(back_rows, group_count, lane_count, group_cap, wide0, wide1)
    first_grad = lax.dot_general(
        arrived, grad_gate, contract_rows, preferred_element_type=jnp.float32
    )
    second_grad = lax.dot_general(
        arrived, grad_up, contract_rows, preferred_element_type=jnp.float32
    )
    third_grad = lax.dot_general(
        weighted, cot_rows, contract_rows, preferred_element_type=jnp.float32
    )
    result = lax.dot_general(pick, returned, contract_rows, preferred_element_type=jnp.float32)
    token_grad = result[:, :piece]
    gate_grad = jnp.sum(jnp.where(named, result[:, None, piece:], 0.0), axis=2)
    gate_grad = gate_grad.astype(jnp.bfloat16).astype(jnp.float32)
    group_grad = jnp.sum(expert_weight * gate_grad, axis=1)
    expert_grad = group_weight[:, None] * gate_grad
    return (
        token_grad,
        group_grad,
        expert_grad,
        first_grad[None],
        second_grad[None],
        third_grad[None],
    )


def solution(mesh):
    lanes = mesh.shape["tp"]
    split = Mesh(mesh.devices.reshape(-1, EPG, lanes), ("g", "e", "tp"))
    ep = ("g", "e")
    in_specs = (
        P(ep, None),
        P(ep, None),
        P(ep),
        P(ep, None),
        P(ep),
        P(ep, None),
        P(ep, None, "tp"),
        P(ep, None, "tp"),
        P(ep, "tp", None),
    )
    out_specs = (
        P(ep, "tp"),
        P(ep),
        P(ep, None),
        P(ep, None, "tp"),
        P(ep, None, "tp"),
        P(ep, "tp", None),
    )
    return jax.shard_map(
        shards, mesh=split, in_specs=in_specs, out_specs=out_specs, check_vma=False
    )
```

profile of v0, /device:TPU:0, one launch (start us, length us, event | category | flops | bytes accessed | tf_op | source)
XLA Modules:
  0.0 107.7 jit_solution(14965847942322609312)
XLA Ops:
  0.6 0.0 copy-start
  0.7 0.8 multiply_convert_fusion.4
  1.4 0.9 convert_reduce_fusion
  2.3 0.7 multiply_add_fusion
  3.0 0.8 fusion.21
  3.8 1.1 constant_dynamic-slice_fusion
  4.9 0.4 convolution_convert_fusion
  5.3 0.6 slice.38.gate_in
  5.9 1.0 fusion.28
  6.9 0.0 copy-start.2
  6.9 48.3 %forward_exchange.1 = (bf16[768,2048]{1,0:T(8,128)(2,1)}, bf16[768,2048]{1,0:T(8,128)(2,1)}, bf16[768,128]{1,0:T(8,128)(2,1)}) custom-call(bf16[192,1024]{1,0:T(8,128)(2,1)} %get-tuple-element.16.tok_in, bf16[192,1024]{1,0:T(8,128)(2,1)} %get-tuple-element.15.cot_in, bf16[192,128]{1,0:T(8,128)(2,1)} %slice.38.gate_in), custom_call_target="tpu_custom_call" | custom-call | tf_op jit(solution)/shard_map/forward_exchange/pallas_call | solution.py:162
  55.2 0.0 copy-start.1
  55.2 1.2 %select_reduce_fusion = f32[768]{0:T(1024)S(1)} fusion(bf16[768,128]{1,0:T(8,128)(2,1)} %get-tuple-element.9, pred[128]{0:T(512)(128)(4,1)S(1)} %iota_compare_fusion.5), kind=kLoop, calls=%fused_computation.31 | loop fusion | flops 294144 | bytes 199808 | tf_op jit(solution)/shard_map/reduce_sum | solution.py:347
  56.5 0.0 copy-done
  56.5 2.9 %fusion.2 = f32[768,256]{0,1:T(8,128)S(1)} fusion(bf16[768,2048]{1,0:T(8,128)(2,1)} %get-tuple-element.11, bf16[1,2048,256]{2,1,0:T(8,128)(2,1)S(1)} %copy-done), kind=kOutput, calls=%fused_computation.7 | convolution fusion | flops 805306368 | bytes 4980736 | tf_op jit(solution)/shard_map/dot_general | solution.py:351
  59.4 0.0 copy-done.2
  59.4 0.0 copy-done.1
  59.4 0.0 copy-start.6
  59.4 0.0 copy-start.7
  59.4 1.1 %fusion.5 = f32[768,256]{0,1:T(8,128)S(1)} fusion(bf16[768,2048]{1,0:T(8,128)(2,1)S(1)} %copy-done.1, bf16[1,2048,256]{2,1,0:T(8,128)(2,1)S(1)} %copy-done.2), kind=kOutput, calls=%fused_computation.10 | convolution fusion | flops 805306368 | bytes 4980736 | tf_op jit(solution)/shard_map/dot_general | solution.py:352
  60.5 0.8 copy-done.6
  61.3 0.3 copy-done.7
  61.6 1.4 %multiply_reduce_fusion = (bf16[768]{0:T(1024)(128)(2,1)S(1)}, bf16[768,256]{0,1:T(8,128)(2,1)S(1)}, bf16[768,256]{0,1:T(8,128)(2,1)S(1)}) fusion(f32[768,256]{0,1:T(8,128)S(1)} %fusion.5, f32[768,256]{0,1:T(8,128)S(1)} %fusion.2, f32[768]{0:T(1024)S(1)} %select_reduce_fusion, bf16[768,2048]{1,0:T(8,128)(2,1)S(1)} %copy-done.6, ...), kind=kOutput, calls=%fused_computation.17 | convolution fusion | flops 808647936 | bytes 6558208 | tf_op jit(solution)/shard_map/dot_general | solution.py:353
  63.0 2.4 %convolution_bitcast_fusion = f32[1,256,2048]{2,1,0:T(8,128)} fusion(bf16[768,2048]{1,0:T(8,128)(2,1)S(1)} %copy-done.6, f32[768]{0:T(1024)S(1)} %select_reduce_fusion, f32[768,256]{0,1:T(8,128)S(1)} %fusion.5, f32[768,256]{0,1:T(8,128)S(1)} %fusion.2), kind=kOutput, calls=%fused_computation.2 | convolution fusion | flops 806682624 | bytes 6818816 | tf_op jit(solution)/shard_map/dot_general | solution.py:385
  65.4 2.4 %convolution_bitcast_fusion.2 = f32[1,2048,256]{2,1,0:T(8,128)} fusion(bf16[768,2048]{1,0:T(8,128)(2,1)S(1)} %copy-done.1, bf16[768,256]{0,1:T(8,128)(2,1)S(1)} %get-tuple-element.13), kind=kOutput, calls=%fused_computation.4 | convolution fusion | flops 805306368 | bytes 5636096 | tf_op jit(solution)/shard_map/dot_general | solution.py:379
  67.8 2.4 %convolution_bitcast_fusion.1 = f32[1,2048,256]{2,1,0:T(8,128)} fusion(bf16[768,2048]{1,0:T(8,128)(2,1)S(1)} %copy-done.1, bf16[768,256]{0,1:T(8,128)(2,1)S(1)} %get-tuple-element.14), kind=kOutput, calls=%fused_computation.3 | convolution fusion | flops 805306368 | bytes 5636096 | tf_op jit(solution)/shard_map/dot_general | solution.py:382
  70.2 1.0 fusion
  71.2 1.0 add_convert_fusion
  72.3 1.1 %slice_dynamic-update-slice_fusion.1 = bf16[768,2304]{1,0:T(8,128)(2,1)} fusion(bf16[768,2048]{1,0:T(8,128)(2,1)S(1)} %add_convert_fusion), kind=kLoop, calls=%fused_computation.15 | loop fusion | bytes 1966080
  73.4 1.1 %slice_dynamic-update-slice_fusion = bf16[768,2304]{1,0:T(8,128)(2,1)} fusion(bf16[768,2304]{1,0:T(8,128)(2,1)} %slice_dynamic-update-slice_fusion.1, bf16[768,2048]{1,0:T(8,128)(2,1)S(1)} %add_convert_fusion), kind=kLoop, calls=%fused_computation.14 | loop fusion | bytes 1966080
  74.5 0.9 slice_dynamic-update-slice_fusion.3
  75.4 0.9 fusion.17
  76.3 0.9 slice_dynamic-update-slice_fusion.2
  77.2 0.9 fusion.18.part
  78.1 0.0 copy-start.3
  78.1 0.0 copy-start.4
  78.1 0.0 copy-start.5
  78.1 26.1 %return_exchange.1 = bf16[192,1152]{1,0:T(8,128)(2,1)} custom-call(bf16[768,2304]{1,0:T(8,128)(2,1)} %fusion.18.part), custom_call_target="tpu_custom_call" | custom-call | tf_op jit(solution)/shard_map/return_exchange/pallas_call | solution.py:289
  104.2 1.3 %fusion.20 = f32[128,1152]{1,0:T(8,128)S(1)} fusion(bf16[192,1152]{1,0:T(8,128)(2,1)} %return_exchange.1, s32[128]{0:T(128)S(1)} %multiply_add_fusion), kind=kOutput, calls=%fused_computation.39 | convolution fusion | flops 56647680 | bytes 1032704 | tf_op jit(solution)/shard_map/dot_general | solution.py:388
  105.6 0.8 slice.43
  106.4 0.0 copy-done.3
  106.4 0.2 select_reduce_fusion.1
  106.6 0.0 copy-done.4
  106.6 0.0 copy-done.5
  106.6 1.1 %convert_multiply_fusion = (f32[128,2]{0,1:T(2,128)}, f32[128]{0:T(128)}) fusion(f32[128]{0:T(128)S(1)} %copy-done.5, bf16[128,2]{0,1:T(2,128)(2,1)S(1)} %select_reduce_fusion.1, f32[128,2]{0,1:T(2,128)S(1)} %copy-done.4), kind=kLoop, calls=%fused_computation.46 | loop fusion | flops 896 | bytes 3584 | tf_op jit(solution)/shard_map/mul | solution.py:393
  (2 shorter events, 0.0 us)
Async XLA Ops:
  0.6 55.8 %copy-start = (bf16[1,2048,256]{2,1,0:T(8,128)(2,1)S(1)}, bf16[1,2048,256]{2,1,0:T(8,128)(2,1)}, u32[]{:S(2)}) copy-start(bf16[1,2048,256]{2,1,0:T(8,128)(2,1)} %param.15) | copy-start | bytes 3145732
  6.9 52.5 %copy-start.2 = (bf16[1,2048,256]{2,1,0:T(8,128)(2,1)S(1)}, bf16[1,2048,256]{2,1,0:T(8,128)(2,1)}, u32[]{:S(2)}) copy-start(bf16[1,2048,256]{2,1,0:T(8,128)(2,1)} %param.16) | copy-start | bytes 3145732
  55.2 4.2 %copy-start.1 = (bf16[768,2048]{1,0:T(8,128)(2,1)S(1)}, bf16[768,2048]{1,0:T(8,128)(2,1)}, u32[]{:S(2)}) copy-start(bf16[768,2048]{1,0:T(8,128)(2,1)} %get-tuple-element.11) | copy-start | bytes 9437188
  59.4 1.9 %copy-start.6 = (bf16[768,2048]{1,0:T(8,128)(2,1)S(1)}, bf16[768,2048]{1,0:T(8,128)(2,1)}, u32[]{:S(2)}) copy-start(bf16[768,2048]{1,0:T(8,128)(2,1)} %get-tuple-element.10) | copy-start | bytes 9437188
  59.4 2.2 %copy-start.7 = (bf16[1,256,2048]{2,1,0:T(8,128)(2,1)S(1)}, bf16[1,256,2048]{2,1,0:T(8,128)(2,1)}, u32[]{:S(2)}) copy-start(bf16[1,256,2048]{2,1,0:T(8,128)(2,1)} %param.17) | copy-start | bytes 3145732
  78.1 28.3 %copy-start.3 = (s32[128,2]{0,1:T(2,128)S(1)}, s32[128,2]{0,1:T(2,128)}, u32[]{:S(2)}) copy-start(s32[128,2]{0,1:T(2,128)} %param.14) | copy-start | bytes 3076
  78.1 28.5 %copy-start.4 = (f32[128,2]{0,1:T(2,128)S(1)}, f32[128,2]{0,1:T(2,128)}, u32[]{:S(2)}) copy-start(f32[128,2]{0,1:T(2,128)} %param.12) | copy-start | bytes 3076
  78.1 28.5 %copy-start.5 = (f32[128]{0:T(128)S(1)}, f32[128]{0:T(128)}, u32[]{:S(2)}) copy-start(f32[128]{0:T(128)} %param.11) | copy-start | bytes 1540
where the time goes:
time: 108 us
  Pallas kernels  74.5 us (69%)
  matrix products  16.4 us (15%)
  local copies, waits for them, and re-layouts  8.69 us (8%)
  other arithmetic  7.36 us (7%)
    pallas_call x1, Pallas kernels, forward(): pl.pallas_call(functools.partial(forward_kernel, groups, lanes, cap, piec...  48.3 us
    pallas_call x1, Pallas kernels, give_back(): pl.pallas_call(functools.partial(return_kernel, groups, lanes, cap, wide0...  26.1 us
    unnamed x20, local copies, waits for them, and re-layouts  5.17 us
    dot_general x1, matrix products, shards(): pre_gate = jnp.dot(arrived, first, preferred_element_type=jnp.float32)  2.9 us
    dot_general x1, matrix products, shards(): lax.dot_general(arrived, grad_up, contract_rows, preferred_element_type=j...  2.41 us
    dot_general x1, matrix products, shards(): lax.dot_general(arrived, grad_gate, contract_rows, preferred_element_type...  2.4 us
    dot_general x1, matrix products, shards(): lax.dot_general(weighted, cot_rows, contract_rows, preferred_element_type...  2.37 us

commit v1 on v0

v1 whole, which is shorter than its diff:
```python
import functools

import jax
import jax.numpy as jnp
from jax import lax
from jax.experimental import pallas as pl
from jax.experimental.pallas import tpu as pltpu
from jax.sharding import Mesh, PartitionSpec as P

EPG = 4
LANES = 128

MESH = pl.DeviceIdType.MESH

CONTRACT_COLS = (((1,), (1,)), ((), ()))
CONTRACT_ROWS = (((0,), (0,)), ((), ()))


def partner(g, d, groups, sign):
    if groups & (groups - 1):
        return lax.rem(g + sign * d + groups, groups)
    met, bit = g, 1
    while bit < groups:
        if d & bit:
            met = met + bit - 2 * bit * ((g // bit) % 2)
        bit *= 2
    return met


class Copies:
    def __init__(self, send_sem, recv_sem):
        self.send_sem, self.recv_sem, self.made = send_sem, recv_sem, []

    def start(self, src, dst, device):
        number = len(self.made)
        copy = pltpu.make_async_remote_copy(
            src_ref=src,
            dst_ref=dst,
            send_sem=self.send_sem.at[number],
            recv_sem=self.recv_sem.at[number],
            device_id=device,
            device_id_type=MESH,
        )
        copy.start()
        self.made.append(copy)
        return copy

    def finish(self):
        for copy in self.made:
            copy.wait_send()


def copy_count(groups, lanes):
    far = lanes - 1
    first = (groups - 1) * 3
    spread = (groups - 1) * (2 + 4 * far) + 2 + 2 * far
    inside = groups * 7
    back = groups * (4 + 2 * far) + groups - 1
    return first + spread + inside + back


def dot(a, b):
    return jnp.dot(a, b, preferred_element_type=jnp.float32)


def add(*parts):
    total = parts[0].astype(jnp.float32)
    for part in parts[1:]:
        total = total + part.astype(jnp.float32)
    return total.astype(jnp.bfloat16)


def plan(groups):
    steps = []
    later = list(range(1, groups))
    steps += [("own", 0), ("arrive", later[0]) if later else ("none", 0), ("relay", 0)]
    for d in later:
        if d > 1:
            steps.append(("arrive", d))
        steps.append(("relay", d))
        steps.append(("inside", d - 1))
        steps.append(("compute", d - 1))
        if d >= 3:
            steps.append(("sum_cores", d - 2))
    last = groups - 1
    steps += [("inside", last), ("compute", last)]
    order = later + [0]
    started = {d for name, d in steps if name == "sum_cores"}
    queue = [d for d in order if d not in started]
    running = [d for d in order if d in started]
    steps += [("sum_cores", d) for d in queue[:1]]
    done = []
    stage = {d: 1 for d in running + queue[:1]}
    waiting = queue[1:]
    while stage or waiting:
        if waiting:
            d = waiting.pop(0)
            steps.append(("sum_cores", d))
            stage[d] = 1
        steps.append(("weights", 0))
        for d in [d for d in order if stage.get(d) == 2][:1]:
            steps.append(("last_sum", d))
            del stage[d]
        for d in [d for d in order if stage.get(d) == 1][:1]:
            steps.append(("middle_sum", d))
            stage[d] = 2
    steps.append(("weights_end", 0))
    return steps


def kernel(
    groups, lanes, cap, wide0, wide1,
    pick, gate_cols, tokens, cotangent, w_gate, w_up, w_down,
    result, grad_first, grad_second, grad_third,
    out_t, out_c, out_g, tok, cot, gate, first, second, third,
    gg, gu, wt, wt_t, part_a, part_b, rc_a, rc_b, s1_a, s1_b, rx_a, rl_a, rl_b, s2_a, s2_b, rx_b,
    done, ret, send, recv, loc,
):
    g, e, y = lax.axis_index("g"), lax.axis_index("e"), lax.axis_index("tp")
    x, c = e // 2, e % 2
    ex, ec = (g, (1 - x) * 2 + c, y), (g, x * 2 + (1 - c), y)
    token_count, feature_count = tokens.shape
    piece = feature_count // lanes
    hidden_count = gg.shape[1]
    rows = EPG * cap
    far = range(1, lanes)
    ahead = [lax.rem(y + r, lanes) for r in far]
    behind = [lax.rem(y + lanes - r, lanes) for r in far]
    others = [(g, e, lane) for lane in ahead]

    barrier = pltpu.get_barrier_semaphore()
    met = [(lax.rem(g + d, groups), e, y) for d in range(1, groups)] + others + [ex, ec]
    for device in met:
        pl.semaphore_signal(barrier, inc=1, device_id=device, device_id_type=MESH)
    loads = [
        pltpu.make_async_copy(src, dst, loc.at[i])
        for i, (src, dst) in enumerate(((w_gate, first), (w_up, second), (w_down, third)))
    ]
    for load in loads:
        load.start()

    chosen = pick[...].reshape(groups * cap, token_count)
    columns = pl.ds(pl.multiple_of(y * piece, LANES), piece)

    def spread_rows(rows_of, source):
        return dot(rows_of, source).astype(jnp.bfloat16)

    out_t[...] = spread_rows(chosen, tokens[:, columns]).reshape(groups, cap, piece)
    out_c[...] = spread_rows(chosen, cotangent[:, columns]).reshape(groups, cap, piece)
    out_g[...] = spread_rows(chosen, gate_cols[...]).reshape(groups, cap, LANES)
    pl.semaphore_wait(barrier, len(met))

    copies = Copies(send, recv)
    state = [dict() for _ in range(groups)]
    for d in range(1, groups):
        target = partner(g, d, groups, -1)
        there = (target, e, y)
        state[d]["zt"] = copies.start(out_t.at[target], tok.at[y, d, 0], there)
        state[d]["zg"] = copies.start(out_g.at[target], gate.at[d, 0], there)
        state[d]["zc"] = copies.start(out_c.at[target], cot.at[y, d, 0], there)

    def own(_):
        s = state[0]
        s["tx"] = [copies.start(out_t.at[g], tok.at[y, 0, 1], ex)]
        s["gx"] = copies.start(out_g.at[g], gate.at[0, 1], ex)
        s["cx"] = copies.start(out_c.at[g], cot.at[y, 0, 1], ex)
        mine = pick[g]
        for lane in range(lanes):
            cols = slice(lane * piece, (lane + 1) * piece)
            tok[lane, 0, 0] = spread_rows(mine, tokens[:, cols])
            cot[lane, 0, 0] = spread_rows(mine, cotangent[:, cols])
        gate[0, 0] = out_g[g]
        s["core"] = [
            copies.start(out_g.at[g], gate.at[0, 2], ec),
            copies.start(tok.at[:, 0, 0], tok.at[:, 0, 2], ec),
            copies.start(cot.at[:, 0, 0], cot.at[:, 0, 2], ec),
        ]

    def arrive(d):
        s = state[d]
        s["zt"].wait_recv()
        mine = tok.at[y, d, 0]
        s["tl"] = [copies.start(mine, mine, device) for device in others]
        s["tx"] = [copies.start(mine, tok.at[y, d, 1], ex)]
        s["zg"].wait_recv()
        s["gx"] = copies.start(gate.at[d, 0], gate.at[d, 1], ex)
        s["core"] = [copies.start(gate.at[d, 0], gate.at[d, 2], ec)]
        s["zc"].wait_recv()
        mine = cot.at[y, d, 0]
        s["cx"] = [copies.start(mine, cot.at[y, d, 1], ex)][0]
        s["cl"] = [copies.start(mine, mine, device) for device in others]

    def relay(d):
        s = state[d]
        if d == 0:
            s["tx"][0].wait_recv()
            theirs = tok.at[y, 0, 1]
            s["txl"] = [copies.start(theirs, theirs, device) for device in others]
        else:
            for i, copy in enumerate(s["tl"]):
                copy.wait_recv()
                theirs = tok.at[behind[i], d, 0]
                s["tx"].append(copies.start(theirs, tok.at[behind[i], d, 1], ex))
            s["core"].append(copies.start(tok.at[:, d, 0], tok.at[:, d, 2], ec))
        s["cx"].wait_recv()
        theirs = cot.at[y, d, 1]
        s["cxl"] = [copies.start(theirs, theirs, device) for device in others]

    def inside(d):
        s = state[d]
        if d == 0:
            for copy in s["txl"]:
                copy.wait_recv()
        else:
            for copy in s["cl"]:
                copy.wait_recv()
            s["core"].append(copies.start(cot.at[:, d, 0], cot.at[:, d, 2], ec))
            for copy in s["tx"]:
                copy.wait_recv()
        s["core"].append(copies.start(tok.at[:, d, 1], tok.at[:, d, 3], ec))
        s["gx"].wait_recv()
        s["core"].append(copies.start(gate.at[d, 1], gate.at[d, 3], ec))
        for copy in s["cxl"]:
            copy.wait_recv()
        s["core"].append(copies.start(cot.at[:, d, 1], cot.at[:, d, 3], ec))

    loaded = []

    def compute(d):
        s = state[d]
        if not loaded:
            for load in loads:
                load.wait()
            loaded.append(True)
        for copy in s["core"]:
            copy.wait_recv()
        pre_gate = pre_up = back = None
        for lane in range(lanes):
            cols = slice(lane * piece, (lane + 1) * piece)
            rows_t = tok[lane, d].reshape(rows, piece)
            rows_c = cot[lane, d].reshape(rows, piece)
            one = dot(rows_t, first[cols, :])
            two = dot(rows_t, second[cols, :])
            three = lax.dot_general(
                rows_c, third[:, cols], CONTRACT_COLS, preferred_element_type=jnp.float32
            )
            pre_gate = one if lane == 0 else pre_gate + one
            pre_up = two if lane == 0 else pre_up + two
            back = three if lane == 0 else back + three
        own_col = lax.broadcasted_iota(jnp.int32, (rows, LANES), 1) == e
        gates = gate[d].reshape(rows, LANES).astype(jnp.float32)
        gate_float = jnp.sum(jnp.where(own_col, gates, 0.0), axis=1, keepdims=True)
        sigma = jax.nn.sigmoid(pre_gate)
        swish = pre_gate * sigma
        hidden = swish * pre_up
        gate_part = jnp.sum(hidden * back, axis=1, keepdims=True)
        scaled = gate_float * back
        grad_gate = (scaled * pre_up * sigma * (1.0 + pre_gate * (1.0 - sigma))).astype(jnp.bfloat16)
        grad_up = (scaled * swish).astype(jnp.bfloat16)
        at = slice(d * rows, (d + 1) * rows)
        gg[at, :] = grad_gate
        gu[at, :] = grad_up
        wt[at, :] = (gate_float * hidden).astype(jnp.bfloat16)
        gate_out = jnp.where(own_col, gate_part, 0.0).astype(jnp.bfloat16)

        def rows_back(lo, hi):
            total = lax.dot_general(
                grad_gate, first[lo:hi, :], CONTRACT_COLS, preferred_element_type=jnp.float32
            ) + lax.dot_general(
                grad_up, second[lo:hi, :], CONTRACT_COLS, preferred_element_type=jnp.float32
            )
            return total.astype(jnp.bfloat16).reshape(EPG, cap, hi - lo)

        for lane in range(lanes):
            lo = lane * piece
            part_a[d, lane] = rows_back(lo, lo + wide0)
            if wide0 < piece:
                part_b[d, lane, :, :, : piece - wide0] = rows_back(lo + wide0, lo + piece)
            part_b[d, lane, :, :, piece - wide0 :] = gate_out.reshape(EPG, cap, LANES)
        s["pa"] = copies.start(part_a.at[d, :, pl.ds(2, 2)], rc_a.at[d], ec)
        s["pb"] = copies.start(part_b.at[d, :, pl.ds(2, 2)], rc_b.at[d], ec)

    def sum_cores(d):
        s = state[d]
        s["pa"].wait_recv()
        s1_a[d] = add(part_a[d, :, 0:2], rc_a[d])
        s["x0"] = copies.start(s1_a.at[d, :, 1], rx_a.at[d], ex)
        s["pb"].wait_recv()
        s1_b[d] = add(part_b[d, :, 0:2], rc_b[d])
        s["l1"] = [
            copies.start(s1_b.at[d, lane], rl_b.at[d, i], (g, e, lane))
            for i, lane in enumerate(ahead)
        ]

    def middle_sum(d):
        s = state[d]
        s["x0"].wait_recv()
        s2_a[d] = add(s1_a[d, :, 0], rx_a[d])
        s["l0"] = [
            copies.start(s2_a.at[d, lane], rl_a.at[d, i], (g, e, lane))
            for i, lane in enumerate(ahead)
        ]
        for copy in s["l1"]:
            copy.wait_recv()
        s2_b[d] = add(s1_b[d, y], *[rl_b[d, i] for i in range(lanes - 1)])
        s["x1"] = copies.start(s2_b.at[d, 1], rx_b.at[d], ex)

    def last_sum(d):
        s = state[d]
        for copy in s["l0"]:
            copy.wait_recv()
        head = add(s2_a[d, y], *[rl_a[d, i] for i in range(lanes - 1)])
        s["x1"].wait_recv()
        tail = add(s2_b[d, 0], rx_b[d])
        if d == 0:
            ret[g, :, :wide0] = head
            ret[g, :, wide0:] = tail
        else:
            done[d, :, :wide0] = head
            done[d, :, wide0:] = tail
            there = (partner(g, d, groups, 1), e, y)
            s["z"] = copies.start(done.at[d], ret.at[g], there)

    tile = min(2 * LANES, piece)
    per = piece // tile
    tiles = feature_count // tile
    seen = [0]

    def weights_to(end):
        if seen[0] == 0 and end > 0:
            wt_t[...] = wt[...].T
        grads_gate, grads_up = gg[...], gu[...]
        left = wt_t[...]

        def turn(i, carry):
            lane, cols = i // per, pl.ds(pl.multiple_of(lax.rem(i, per) * tile, LANES), tile)
            turned = tok[lane, :, :, :, cols].reshape(groups * rows, tile).T
            at = pl.ds(pl.multiple_of(i * tile, LANES), tile)
            grad_first[at, :] = dot(turned, grads_gate)
            grad_second[at, :] = dot(turned, grads_up)
            grad_third[:, at] = dot(left, cot[lane, :, :, :, cols].reshape(groups * rows, tile))
            return carry

        if end > seen[0]:
            lax.fori_loop(seen[0], end, turn, 0)
        seen[0] = end

    steps = plan(groups)
    shares = sum(name == "weights" for name, _ in steps)
    served = [0]

    def weights(_):
        served[0] += 1
        weights_to(tiles * served[0] // shares)

    def weights_end(_):
        weights_to(tiles)

    phases = {
        "own": own, "arrive": arrive, "relay": relay, "inside": inside, "compute": compute,
        "sum_cores": sum_cores, "middle_sum": middle_sum, "last_sum": last_sum,
        "weights": weights, "weights_end": weights_end,
    }
    for name, d in steps:
        if name in phases:
            phases[name](d)
    for d in range(1, groups):
        state[d]["z"].wait_recv()
    result[...] = lax.dot_general(
        chosen,
        ret[...].reshape(groups * cap, wide0 + wide1),
        CONTRACT_ROWS,
        preferred_element_type=jnp.float32,
    )
    copies.finish()


def route(pick, gate_cols, tokens, cotangent, w_gate, w_up, w_down, groups, lanes, cap):
    token_count, feature_count = tokens.shape
    hidden_count = w_gate.shape[1]
    piece = feature_count // lanes
    wide1 = (piece + LANES) // (2 * LANES) * LANES
    wide0 = piece + LANES - wide1
    rows = EPG * cap
    far = max(lanes - 1, 1)
    count = copy_count(groups, lanes)
    vmem, hbm = pl.BlockSpec(memory_space=pltpu.VMEM), pl.BlockSpec(memory_space=pl.ANY)

    def buffer(*shape):
        return pltpu.VMEM(shape, jnp.bfloat16)

    def grad(*shape):
        return jax.ShapeDtypeStruct(shape, jnp.float32)

    return pl.pallas_call(
        functools.partial(kernel, groups, lanes, cap, wide0, wide1),
        out_shape=(
            grad(token_count, wide0 + wide1),
            grad(feature_count, hidden_count),
            grad(feature_count, hidden_count),
            grad(hidden_count, feature_count),
        ),
        in_specs=[vmem] * 4 + [hbm] * 3,
        out_specs=(vmem,) * 4,
        scratch_shapes=[
            buffer(groups, cap, piece),
            buffer(groups, cap, piece),
            buffer(groups, cap, LANES),
            buffer(lanes, groups, EPG, cap, piece),
            buffer(lanes, groups, EPG, cap, piece),
            buffer(groups, EPG, cap, LANES),
            buffer(feature_count, hidden_count),
            buffer(feature_count, hidden_count),
            buffer(hidden_count, feature_count),
            buffer(groups * rows, hidden_count),
            buffer(groups * rows, hidden_count),
            buffer(groups * rows, hidden_count),
            buffer(hidden_count, groups * rows),
            buffer(groups, lanes, EPG, cap, wide0),
            buffer(groups, lanes, EPG, cap, wide1),
            buffer(groups, lanes, 2, cap, wide0),
            buffer(groups, lanes, 2, cap, wide1),
            buffer(groups, lanes, 2, cap, wide0),
            buffer(groups, lanes, 2, cap, wide1),
            buffer(groups, lanes, cap, wide0),
            buffer(groups, far, cap, wide0),
            buffer(groups, far, 2, cap, wide1),
            buffer(groups, lanes, cap, wide0),
            buffer(groups, 2, cap, wide1),
            buffer(groups, cap, wide1),
            buffer(groups, cap, wide0 + wide1),
            buffer(groups, cap, wide0 + wide1),
            pltpu.SemaphoreType.DMA((count,)),
            pltpu.SemaphoreType.DMA((count,)),
            pltpu.SemaphoreType.DMA((3,)),
        ],
        compiler_params=pltpu.CompilerParams(
            collective_id=0, has_side_effects=True, vmem_limit_bytes=60 * 1024 * 1024
        ),
        name="routed_backward",
    )(pick, gate_cols, tokens, cotangent, w_gate, w_up, w_down)


def shards(
    tokens, cotangent, group_weight, expert_weight, group_choice, local_choice, w_gate, w_up, w_down
):
    token_count, feature_count = tokens.shape
    pick_count = expert_weight.shape[1]
    group_count = lax.axis_size("g")
    lane_count = lax.axis_size("tp")
    expert_count = group_count * EPG
    capacity = pick_count * (3 * token_count // (2 * expert_count))
    group_cap = -(-(EPG * capacity // pick_count) // 16) * 16
    row_count = group_count * group_cap
    piece = feature_count // lane_count
    order = jnp.arange(token_count, dtype=jnp.int32)
    same = (group_choice[:, None] == group_choice[None, :]) & (order[:, None] > order[None, :])
    dest = group_choice * group_cap + jnp.sum(same.astype(jnp.int32), axis=1)
    pick = (jnp.arange(row_count, dtype=jnp.int32)[:, None] == dest[None, :]).astype(jnp.bfloat16)
    gate = (group_weight[:, None] * expert_weight).astype(jnp.bfloat16)
    named = local_choice[:, :, None] == jnp.arange(LANES, dtype=jnp.int32)
    gate_cols = jnp.sum(jnp.where(named, gate[:, :, None], 0), axis=1).astype(jnp.bfloat16)
    result, first_grad, second_grad, third_grad = route(
        pick.reshape(group_count, group_cap, token_count),
        gate_cols,
        tokens,
        cotangent,
        w_gate[0],
        w_up[0],
        w_down[0],
        group_count,
        lane_count,
        group_cap,
    )
    token_grad = result[:, :piece]
    gate_grad = jnp.sum(jnp.where(named, result[:, None, piece:], 0.0), axis=2)
    gate_grad = gate_grad.astype(jnp.bfloat16).astype(jnp.float32)
    group_grad = jnp.sum(expert_weight * gate_grad, axis=1)
    expert_grad = group_weight[:, None] * gate_grad
    return (
        token_grad,
        group_grad,
        expert_grad,
        first_grad[None],
        second_grad[None],
        third_grad[None],
    )


def solution(mesh):
    lanes = mesh.shape["tp"]
    split = Mesh(mesh.devices.reshape(-1, EPG, lanes), ("g", "e", "tp"))
    ep = ("g", "e")
    in_specs = (
        P(ep, None),
        P(ep, None),
        P(ep),
        P(ep, None),
        P(ep),
        P(ep, None),
        P(ep, None, "tp"),
        P(ep, None, "tp"),
        P(ep, "tp", None),
    )
    out_specs = (
        P(ep, "tp"),
        P(ep),
        P(ep, None),
        P(ep, None, "tp"),
        P(ep, None, "tp"),
        P(ep, "tp", None),
    )
    return jax.shard_map(
        shards, mesh=split, in_specs=in_specs, out_specs=out_specs, check_vma=False
    )
```

time: 108 us -> 95 us (0.88)
  matrix products: 16.4 us -> 0 us
  Pallas kernels: 74.5 us -> 78.7 us
  other arithmetic: 7.36 us -> 5.66 us
    dot_general x10 -> x0, matrix products: 16.4 us -> none  [the longest x1 2.9 us: shards(): pre_gate = jnp.dot(arrived, first, preferred_element_type=jnp.float32)]
    pallas_call x2 -> x1, Pallas kernels: 74.5 us -> 78.7 us  [route(): pl.pallas_call(functools.partial(kernel, groups, lanes, cap, wide0, wide1...]
    unnamed x20 -> x13, local copies, waits for them, and re-layouts: 5.17 us -> 6.87 us
    slice x2 -> x0, local copies, waits for them, and re-layouts: 1.6 us -> none  [the longest x1 0.98 us: shards(): rows[:, piece:2 * piece]]
    reduce_sum x1 -> x0, other arithmetic: 1.22 us -> none  [shards(): gate_float = jnp.sum(jnp.where(own, gate_block, 0.0), axis=1, keepdims=True)]
where the time goes in v1:
time: 95 us; the launch traced here: 94.7 us
  Pallas kernels  78.7 us (83%)
  local copies, waits for them, and re-layouts  9.6 us (10%)
  other arithmetic  5.66 us (6%)
    pallas_call x1, Pallas kernels, route(): pl.pallas_call(functools.partial(kernel, groups, lanes, cap, wide0, wide1...  78.7 us
    unnamed x13, local copies, waits for them, and re-layouts  6.87 us

profile of v1, /device:TPU:0, one launch (start us, length us, event | category | flops | bytes accessed | tf_op | source)
XLA Modules:
  0.0 94.7 jit_solution(13005024729900635849)
XLA Ops:
  0.6 0.9 convert_reduce_fusion
  1.5 0.7 multiply_add_fusion.1
  2.2 0.7 compare_convert_fusion.pick
  2.9 0.7 multiply_convert_fusion
  3.6 1.4 %fusion.1.gate_cols = bf16[128,128]{1,0:T(8,128)(2,1)} fusion(s32[128,2]{0,1:T(2,128)} %param.14, bf16[128,2]{0,1:T(2,128)(2,1)S(1)} %multiply_convert_fusion), kind=kLoop, calls=%fused_computation.4 | loop fusion | flops 81920 | bytes 34304 | tf_op jit(solution)/shard_map/reduce_sum | solution.py:462
  5.1 0.0 copy-start.2
  5.1 0.0 copy-start.3
  5.1 0.0 copy-start.4
  5.1 78.7 %routed_backward.1 = (f32[128,1152]{1,0:T(8,128)}, f32[2048,256]{1,0:T(8,128)}, f32[2048,256]{1,0:T(8,128)}, f32[256,2048]{1,0:T(8,128)}) custom-call(bf16[4,48,128]{2,1,0:T(8,128)(2,1)} %compare_convert_fusion.pick, bf16[128,128]{1,0:T(8,128)(2,1)} %fusion.1.gate_cols, bf16[128,2048]{1,0:T(8,128)(2,1)} %tokens.1, bf16[128,2048]{1,0:T(8,128)(2,1)} %cotangent.1, ...), custom_call_target="tpu_custom_call" | custom-call | tf_op jit(solution)/shard_map/routed_backward/pallas_call | solution.py:395
  83.8 0.8 slice.7
  84.6 0.0 copy-done.2
  84.6 0.2 select_reduce_fusion
  84.8 0.0 copy-done.3
  84.8 0.0 copy-done.4
  84.8 1.1 %convert_multiply_fusion = (f32[128,2]{0,1:T(2,128)}, f32[128]{0:T(128)}) fusion(f32[128]{0:T(128)S(1)} %copy-done.4, bf16[128,2]{0,1:T(2,128)(2,1)S(1)} %select_reduce_fusion, f32[128,2]{0,1:T(2,128)S(1)} %copy-done.3), kind=kLoop, calls=%fused_computation.9 | loop fusion | flops 896 | bytes 3584 | tf_op jit(solution)/shard_map/mul | solution.py:479
  85.9 1.9 %slice.6 = f32[128,1024]{1,0:T(8,128)} slice(f32[128,1152]{1,0:T(8,128)} %get-tuple-element.10), slice={[0:128], [0:1024]} | slice | bytes 1048576 | tf_op jit(solution)/shard_map/slice | solution.py:475
  87.8 0.0 copy-start.1
  87.8 3.2 %copy.20 = f32[1,2048,256]{2,1,0:T(8,128)} copy(f32[1,2048,256]{2,1,0:T(8,128)} %bitcast.8) | data formatting | bytes 4194304
  91.0 0.0 copy-done.1
  91.0 0.0 copy-start
  91.0 1.3 %copy.21 = f32[1,2048,256]{2,1,0:T(8,128)} copy(f32[1,2048,256]{2,1,0:T(8,128)S(1)} %bitcast.7) | data formatting | bytes 4194304
  92.3 1.0 %copy-done = f32[256,2048]{1,0:T(8,128)S(1)} copy-done((f32[256,2048]{1,0:T(8,128)S(1)}, f32[256,2048]{1,0:T(8,128)}, u32[]{:S(2)}) %copy-start) | copy-done | bytes 2097176
  93.3 1.3 %copy.22 = f32[1,256,2048]{2,1,0:T(8,128)} copy(f32[1,256,2048]{2,1,0:T(8,128)S(1)} %bitcast.6) | data formatting | bytes 4194304
  (1 shorter events, 0.0 us)
Async XLA Ops:
  5.1 79.6 %copy-start.2 = (s32[128,2]{0,1:T(2,128)S(1)}, s32[128,2]{0,1:T(2,128)}, u32[]{:S(2)}) copy-start(s32[128,2]{0,1:T(2,128)} %param.14) | copy-start | bytes 3076
  5.1 79.8 %copy-start.3 = (f32[128,2]{0,1:T(2,128)S(1)}, f32[128,2]{0,1:T(2,128)}, u32[]{:S(2)}) copy-start(f32[128,2]{0,1:T(2,128)} %param.12) | copy-start | bytes 3076
  5.1 79.8 %copy-start.4 = (f32[128]{0:T(128)S(1)}, f32[128]{0:T(128)}, u32[]{:S(2)}) copy-start(f32[128]{0:T(128)} %param.11) | copy-start | bytes 1540
  87.8 3.2 %copy-start.1 = (f32[2048,256]{1,0:T(8,128)S(1)}, f32[2048,256]{1,0:T(8,128)}, u32[]{:S(2)}) copy-start(f32[2048,256]{1,0:T(8,128)} %get-tuple-element.12) | copy-start | bytes 6291460
  91.0 2.3 %copy-start = (f32[256,2048]{1,0:T(8,128)S(1)}, f32[256,2048]{1,0:T(8,128)}, u32[]{:S(2)}) copy-start(f32[256,2048]{1,0:T(8,128)} %get-tuple-element.13) | copy-start | bytes 6291460

commit v2 on v1

--- a/solution.py
+++ b/solution.py
@@ -9,6 +9,8 @@
 
 EPG = 4
 LANES = 128
+VMEM_LIMIT = 36 * 1024 * 1024
+FINISH_LIMIT = 16 * 1024 * 1024
 
 MESH = pl.DeviceIdType.MESH
 
@@ -27,13 +29,16 @@
     return met
 
 
+def swapped(g, groups):
+    return 0 if groups & (groups - 1) else (g + g // 2) % 2
+
+
 class Copies:
     def __init__(self, send_sem, recv_sem):
-        self.send_sem, self.recv_sem, self.made = send_sem, recv_sem, []
-
-    def start(self, src, dst, device):
-        number = len(self.made)
-        copy = pltpu.make_async_remote_copy(
+        self.send_sem, self.recv_sem, self.count, self.made = send_sem, recv_sem, 0, []
+
+    def describe(self, src, dst, device, number):
+        return pltpu.make_async_remote_copy(
             src_ref=src,
             dst_ref=dst,
             send_sem=self.send_sem.at[number],
@@ -41,6 +46,13 @@
             device_id=device,
             device_id_type=MESH,
         )
+
+    def reserve(self, count):
+        self.count += count
+        return self.count - count
+
+    def start(self, src, dst, device):
+        copy = self.describe(src, dst, device, self.reserve(1))
         copy.start()
         self.made.append(copy)
         return copy
@@ -71,27 +83,29 @@
 
 
 def plan(groups):
-    steps = []
-    later = list(range(1, groups))
-    steps += [("own", 0), ("arrive", later[0]) if later else ("none", 0), ("relay", 0)]
-    for d in later:
+    steps = [("own", 0), ("relay_t", 0)]
+    if groups > 1:
+        steps += [("arrive_t", 1), ("relay_c", 0), ("arrive_c", 1), ("relay_t", 1), ("relay_c", 1)]
+    else:
+        steps += [("relay_c", 0), ("inside_t", 0), ("inside_c", 0), ("compute", 0)]
+    for d in range(1, groups):
+        more = d + 1 < groups
+        if more:
+            steps.append(("arrive_t", d + 1))
+        if d == 1:
+            steps += [("inside_t", 0), ("inside_c", 0), ("compute", 0)]
+        steps.append(("inside_t", d))
+        if more:
+            steps.append(("arrive_c", d + 1))
+        steps.append(("inside_c", d))
+        if more:
+            steps += [("relay_t", d + 1), ("relay_c", d + 1)]
+        steps.append(("compute", d))
         if d > 1:
-            steps.append(("arrive", d))
-        steps.append(("relay", d))
-        steps.append(("inside", d - 1))
-        steps.append(("compute", d - 1))
-        if d >= 3:
-            steps.append(("sum_cores", d - 2))
-    last = groups - 1
-    steps += [("inside", last), ("compute", last)]
-    order = later + [0]
-    started = {d for name, d in steps if name == "sum_cores"}
-    queue = [d for d in order if d not in started]
-    running = [d for d in order if d in started]
-    steps += [("sum_cores", d) for d in queue[:1]]
-    done = []
-    stage = {d: 1 for d in running + queue[:1]}
-    waiting = queue[1:]
+            steps.append(("sum_cores", d - 1))
+    order = list(range(1, groups)) + [0]
+    stage = {d: 1 for d in range(1, groups - 1)}
+    waiting = [d for d in order if d not in stage]
     while stage or waiting:
         if waiting:
             d = waiting.pop(0)
@@ -104,15 +118,14 @@
         for d in [d for d in order if stage.get(d) == 1][:1]:
             steps.append(("middle_sum", d))
             stage[d] = 2
-    steps.append(("weights_end", 0))
     return steps
 
 
 def kernel(
     groups, lanes, cap, wide0, wide1,
-    pick, gate_cols, tokens, cotangent, w_gate, w_up, w_down,
-    result, grad_first, grad_second, grad_third,
-    out_t, out_c, out_g, tok, cot, gate, first, second, third,
+    choice_in, weight_in, weights_in, local_in, tokens_in, cotangent_in, w_gate, w_up, w_down,
+    token_grad, gate_grad, grad_first, grad_second, grad_third,
+    choice, weight, weights_t, local_t, tokens, cotangent, pick, out_t, out_c, out_g, tok, cot, gate, first, second, third,
     gg, gu, wt, wt_t, part_a, part_b, rc_a, rc_b, s1_a, s1_b, rx_a, rl_a, rl_b, s2_a, s2_b, rx_b,
     done, ret, send, recv, loc,
 ):
@@ -121,43 +134,89 @@
     ex, ec = (g, (1 - x) * 2 + c, y), (g, x * 2 + (1 - c), y)
     token_count, feature_count = tokens.shape
     piece = feature_count // lanes
-    hidden_count = gg.shape[1]
     rows = EPG * cap
     far = range(1, lanes)
     ahead = [lax.rem(y + r, lanes) for r in far]
     behind = [lax.rem(y + lanes - r, lanes) for r in far]
     others = [(g, e, lane) for lane in ahead]
 
+    loads = [
+        pltpu.make_async_copy(src, dst, loc.at[i])
+        for i, (src, dst) in enumerate(
+            (
+                (choice_in, choice), (weight_in, weight), (weights_in, weights_t),
+                (local_in, local_t), (tokens_in, tokens), (cotangent_in, cotangent),
+                (w_gate, first), (w_up, second), (w_down, third),
+            )
+        )
+    ]
+    for load in loads:
+        load.start()
     barrier = pltpu.get_barrier_semaphore()
     met = [(lax.rem(g + d, groups), e, y) for d in range(1, groups)] + others + [ex, ec]
     for device in met:
         pl.semaphore_signal(barrier, inc=1, device_id=device, device_id_type=MESH)
-    loads = [
-        pltpu.make_async_copy(src, dst, loc.at[i])
-        for i, (src, dst) in enumerate(((w_gate, first), (w_up, second), (w_down, third)))
-    ]
-    for load in loads:
-        load.start()
-
-    chosen = pick[...].reshape(groups * cap, token_count)
-    columns = pl.ds(pl.multiple_of(y * piece, LANES), piece)
+
+    def iota(shape, dim):
+        return lax.broadcasted_iota(jnp.int32, shape, dim)
 
     def spread_rows(rows_of, source):
         return dot(rows_of, source).astype(jnp.bfloat16)
 
-    out_t[...] = spread_rows(chosen, tokens[:, columns]).reshape(groups, cap, piece)
-    out_c[...] = spread_rows(chosen, cotangent[:, columns]).reshape(groups, cap, piece)
-    out_g[...] = spread_rows(chosen, gate_cols[...]).reshape(groups, cap, LANES)
+    for load in loads[:4]:
+        load.wait()
+    chosen = choice[...]
+    square = (token_count, token_count)
+    earlier = (iota(square, 0) < iota(square, 1)).astype(jnp.float32).astype(jnp.bfloat16)
+    high = -(-groups // 16) * 16
+    named = iota((high, token_count), 0) == chosen
+    member = jnp.where(named, 1.0, 0.0)
+    rank = jnp.sum(member * dot(member.astype(jnp.bfloat16), earlier), axis=0, keepdims=True)
+    rank = jnp.where(rank < cap, rank, cap).astype(jnp.int32)
+    dest = chosen * cap + rank
+    one_hot = jnp.where(iota((groups * cap, token_count), 0) == dest, 1.0, 0.0).astype(jnp.bfloat16)
+    pick[...] = one_hot.reshape(groups, cap, token_count)
+    gates = (weight[...] * weights_t[...]).astype(jnp.bfloat16).astype(jnp.float32)
+    gate_rows = jnp.zeros((LANES, token_count), jnp.float32)
+    for k in range(local_t.shape[0]):
+        hit = iota((LANES, token_count), 0) == local_t[k : k + 1, :]
+        gate_rows = gate_rows + jnp.where(hit, gates[k : k + 1, :], 0.0)
+    columns = pl.ds(pl.multiple_of(y * piece, LANES), piece)
+    blocks = lax.dot_general(
+        one_hot, gate_rows.astype(jnp.bfloat16), CONTRACT_COLS, preferred_element_type=jnp.float32
+    )
+    out_g[...] = blocks.astype(jnp.bfloat16).reshape(groups, cap, LANES)
+    loads[4].wait()
+    out_t[...] = spread_rows(one_hot, tokens[:, columns]).reshape(groups, cap, piece)
+    loads[5].wait()
+    out_c[...] = spread_rows(one_hot, cotangent[:, columns]).reshape(groups, cap, piece)
     pl.semaphore_wait(barrier, len(met))
 
     copies = Copies(send, recv)
     state = [dict() for _ in range(groups)]
+    base = copies.reserve(3 * (groups - 1))
+    flip = swapped(g, groups)
+
+    def cross(d, target):
+        there = (target, e, y)
+        number = base + 3 * (d - 1)
+        return [
+            copies.describe(out_t.at[target], tok.at[y, d, 0], there, number),
+            copies.describe(out_g.at[target], gate.at[d, 0], there, number + 1),
+            copies.describe(out_c.at[target], cot.at[y, d, 0], there, number + 2),
+        ]
+
+    for k in range(1, groups):
+        d, target = k, partner(g, k, groups, -1)
+        if k > 1 and not isinstance(flip, int):
+            d = k + flip * (1 - 2 * (k % 2))
+            target = target + flip * (1 - 2 * (target % 2))
+        for copy in cross(d, target):
+            copy.start()
     for d in range(1, groups):
-        target = partner(g, d, groups, -1)
-        there = (target, e, y)
-        state[d]["zt"] = copies.start(out_t.at[target], tok.at[y, d, 0], there)
-        state[d]["zg"] = copies.start(out_g.at[target], gate.at[d, 0], there)
-        state[d]["zc"] = copies.start(out_c.at[target], cot.at[y, d, 0], there)
+        arriving = cross(d, partner(g, d, groups, -1))
+        copies.made += arriving
+        state[d]["zt"], state[d]["zg"], state[d]["zc"] = arriving
 
     def own(_):
         s = state[0]
@@ -176,7 +235,7 @@
             copies.start(cot.at[:, 0, 0], cot.at[:, 0, 2], ec),
         ]
 
-    def arrive(d):
+    def arrive_t(d):
         s = state[d]
         s["zt"].wait_recv()
         mine = tok.at[y, d, 0]
@@ -185,12 +244,15 @@
         s["zg"].wait_recv()
         s["gx"] = copies.start(gate.at[d, 0], gate.at[d, 1], ex)
         s["core"] = [copies.start(gate.at[d, 0], gate.at[d, 2], ec)]
+
+    def arrive_c(d):
+        s = state[d]
         s["zc"].wait_recv()
         mine = cot.at[y, d, 0]
-        s["cx"] = [copies.start(mine, cot.at[y, d, 1], ex)][0]
+        s["cx"] = copies.start(mine, cot.at[y, d, 1], ex)
         s["cl"] = [copies.start(mine, mine, device) for device in others]
 
-    def relay(d):
+    def relay_t(d):
         s = state[d]
         if d == 0:
             s["tx"][0].wait_recv()
@@ -202,11 +264,14 @@
                 theirs = tok.at[behind[i], d, 0]
                 s["tx"].append(copies.start(theirs, tok.at[behind[i], d, 1], ex))
             s["core"].append(copies.start(tok.at[:, d, 0], tok.at[:, d, 2], ec))
+
+    def relay_c(d):
+        s = state[d]
         s["cx"].wait_recv()
         theirs = cot.at[y, d, 1]
         s["cxl"] = [copies.start(theirs, theirs, device) for device in others]
 
-    def inside(d):
+    def inside_t(d):
         s = state[d]
         if d == 0:
             for copy in s["txl"]:
@@ -218,6 +283,9 @@
             for copy in s["tx"]:
                 copy.wait_recv()
         s["core"].append(copies.start(tok.at[:, d, 1], tok.at[:, d, 3], ec))
+
+    def inside_c(d):
+        s = state[d]
         s["gx"].wait_recv()
         s["core"].append(copies.start(gate.at[d, 1], gate.at[d, 3], ec))
         for copy in s["cxl"]:
@@ -229,7 +297,7 @@
     def compute(d):
         s = state[d]
         if not loaded:
-            for load in loads:
+            for load in loads[6:]:
                 load.wait()
             loaded.append(True)
         for copy in s["core"]:
@@ -247,7 +315,7 @@
             pre_gate = one if lane == 0 else pre_gate + one
             pre_up = two if lane == 0 else pre_up + two
             back = three if lane == 0 else back + three
-        own_col = lax.broadcasted_iota(jnp.int32, (rows, LANES), 1) == e
+        own_col = iota((rows, LANES), 1) == e
         gates = gate[d].reshape(rows, LANES).astype(jnp.float32)
         gate_float = jnp.sum(jnp.where(own_col, gates, 0.0), axis=1, keepdims=True)
         sigma = jax.nn.sigmoid(pre_gate)
@@ -353,29 +421,29 @@
         served[0] += 1
         weights_to(tiles * served[0] // shares)
 
-    def weights_end(_):
-        weights_to(tiles)
-
     phases = {
-        "own": own, "arrive": arrive, "relay": relay, "inside": inside, "compute": compute,
+        "own": own, "arrive_t": arrive_t, "arrive_c": arrive_c, "relay_t": relay_t,
+        "relay_c": relay_c, "inside_t": inside_t, "inside_c": inside_c, "compute": compute,
         "sum_cores": sum_cores, "middle_sum": middle_sum, "last_sum": last_sum,
-        "weights": weights, "weights_end": weights_end,
+        "weights": weights,
     }
     for name, d in steps:
-        if name in phases:
+        with jax.named_scope(f"{name}_{d}"):
             phases[name](d)
-    for d in range(1, groups):
-        state[d]["z"].wait_recv()
-    result[...] = lax.dot_general(
-        chosen,
-        ret[...].reshape(groups * cap, wide0 + wide1),
-        CONTRACT_ROWS,
-        preferred_element_type=jnp.float32,
-    )
+    with jax.named_scope("gather"):
+        for d in range(1, groups):
+            state[d]["z"].wait_recv()
+        back = ret[...].reshape(groups * cap, wide0 + wide1)
+        token_grad[...] = lax.dot_general(
+            one_hot, back[:, :piece], CONTRACT_ROWS, preferred_element_type=jnp.float32
+        )
+        gate_grad[...] = lax.dot_general(
+            back[:, piece:], one_hot, CONTRACT_ROWS, preferred_element_type=jnp.float32
+        )
     copies.finish()
 
 
-def route(pick, gate_cols, tokens, cotangent, w_gate, w_up, w_down, groups, lanes, cap):
+def route(choice, weight, weights_t, local_t, tokens, cotangent, w_gate, w_up, w_down, groups, lanes, cap):
     token_count, feature_count = tokens.shape
     hidden_count = w_gate.shape[1]
     piece = feature_count // lanes
@@ -384,7 +452,7 @@
     rows = EPG * cap
     far = max(lanes - 1, 1)
     count = copy_count(groups, lanes)
-    vmem, hbm = pl.BlockSpec(memory_space=pltpu.VMEM), pl.BlockSpec(memory_space=pl.ANY)
+    vmem, hbm = pl.BlockSpec(memory_space=pltpu.VMEM), pl.BlockSpec(memory_space=pltpu.HBM)
 
     def buffer(*shape):
         return pltpu.VMEM(shape, jnp.bfloat16)
@@ -395,14 +463,22 @@
     return pl.pallas_call(
         functools.partial(kernel, groups, lanes, cap, wide0, wide1),
         out_shape=(
-            grad(token_count, wide0 + wide1),
+            grad(token_count, piece),
+            grad(LANES, token_count),
             grad(feature_count, hidden_count),
             grad(feature_count, hidden_count),
             grad(hidden_count, feature_count),
         ),
-        in_specs=[vmem] * 4 + [hbm] * 3,
-        out_specs=(vmem,) * 4,
+        in_specs=[hbm] * 9,
+        out_specs=(vmem,) * 5,
         scratch_shapes=[
+            pltpu.VMEM(choice.shape, choice.dtype),
+            pltpu.VMEM(weight.shape, weight.dtype),
+            pltpu.VMEM(weights_t.shape, weights_t.dtype),
+            pltpu.VMEM(local_t.shape, local_t.dtype),
+            buffer(token_count, feature_count),
+            buffer(token_count, feature_count),
+            buffer(groups, cap, token_count),
             buffer(groups, cap, piece),
             buffer(groups, cap, piece),
             buffer(groups, cap, LANES),
@@ -432,55 +508,89 @@
             buffer(groups, cap, wide0 + wide1),
             pltpu.SemaphoreType.DMA((count,)),
             pltpu.SemaphoreType.DMA((count,)),
-            pltpu.SemaphoreType.DMA((3,)),
+            pltpu.SemaphoreType.DMA((9,)),
         ],
         compiler_params=pltpu.CompilerParams(
-            collective_id=0, has_side_effects=True, vmem_limit_bytes=60 * 1024 * 1024
+            collective_id=0, has_side_effects=True, vmem_limit_bytes=VMEM_LIMIT
         ),
         name="routed_backward",
-    )(pick, gate_cols, tokens, cotangent, w_gate, w_up, w_down)
+    )(choice, weight, weights_t, local_t, tokens, cotangent, w_gate, w_up, w_down)
+
+
+def finish_kernel(
+    weight, weights_t, local_t, gate_grad, token_grad, first, second, third,
+    group_out, expert_out, token_out, first_out, second_out, third_out, sem,
+):
+    moves = [
+        pltpu.make_async_copy(src, dst, sem.at[i])
+        for i, (src, dst) in enumerate(
+            (
+                (first, first_out), (second, second_out), (third, third_out),
+                (token_grad, token_out),
+            )
+        )
+    ]
+    for move in moves:
+        move.start()
+    total = None
+    for k in range(local_t.shape[0]):
+        hit = lax.broadcasted_iota(jnp.int32, gate_grad.shape, 0) == local_t[k : k + 1, :]
+        held = jnp.sum(jnp.where(hit, gate_grad[...], 0.0), axis=0, keepdims=True)
+        held = held.astype(jnp.bfloat16).astype(jnp.float32)
+        expert_out[k : k + 1, :] = weight[...] * held
+        term = weights_t[k : k + 1, :] * held
+        total = term if total is None else total + term
+    group_out[...] = total
+    for move in moves:
+        move.wait()
+
+
+def finish(weight, weights_t, local_t, gate_grad, token_grad, first, second, third):
+    vmem, hbm = pl.BlockSpec(memory_space=pltpu.VMEM), pl.BlockSpec(memory_space=pltpu.HBM)
+
+    def like(array):
+        return jax.ShapeDtypeStruct(array.shape, jnp.float32)
+
+    return pl.pallas_call(
+        finish_kernel,
+        out_shape=(
+            like(weight), like(weights_t), like(token_grad), like(first), like(second), like(third)
+        ),
+        in_specs=[vmem] * 8,
+        out_specs=(vmem,) * 2 + (hbm,) * 4,
+        scratch_shapes=[pltpu.SemaphoreType.DMA((4,))],
+        compiler_params=pltpu.CompilerParams(vmem_limit_bytes=FINISH_LIMIT),
+        name="write_results",
+    )(weight, weights_t, local_t, gate_grad, token_grad, first, second, third)
 
 
 def shards(
     tokens, cotangent, group_weight, expert_weight, group_choice, local_choice, w_gate, w_up, w_down
 ):
-    token_count, feature_count = tokens.shape
+    token_count = tokens.shape[0]
     pick_count = expert_weight.shape[1]
     group_count = lax.axis_size("g")
     lane_count = lax.axis_size("tp")
     expert_count = group_count * EPG
     capacity = pick_count * (3 * token_count // (2 * expert_count))
     group_cap = -(-(EPG * capacity // pick_count) // 16) * 16
-    row_count = group_count * group_cap
-    piece = feature_count // lane_count
-    order = jnp.arange(token_count, dtype=jnp.int32)
-    same = (group_choice[:, None] == group_choice[None, :]) & (order[:, None] > order[None, :])
-    dest = group_choice * group_cap + jnp.sum(same.astype(jnp.int32), axis=1)
-    pick = (jnp.arange(row_count, dtype=jnp.int32)[:, None] == dest[None, :]).astype(jnp.bfloat16)
-    gate = (group_weight[:, None] * expert_weight).astype(jnp.bfloat16)
-    named = local_choice[:, :, None] == jnp.arange(LANES, dtype=jnp.int32)
-    gate_cols = jnp.sum(jnp.where(named, gate[:, :, None], 0), axis=1).astype(jnp.bfloat16)
-    result, first_grad, second_grad, third_grad = route(
-        pick.reshape(group_count, group_cap, token_count),
-        gate_cols,
-        tokens,
-        cotangent,
-        w_gate[0],
-        w_up[0],
-        w_down[0],
-        group_count,
-        lane_count,
-        group_cap,
-    )
-    token_grad = result[:, :piece]
-    gate_grad = jnp.sum(jnp.where(named, result[:, None, piece:], 0.0), axis=2)
-    gate_grad = gate_grad.astype(jnp.bfloat16).astype(jnp.float32)
-    group_grad = jnp.sum(expert_weight * gate_grad, axis=1)
-    expert_grad = group_weight[:, None] * gate_grad
+    weight = group_weight.reshape(1, token_count)
+    weights_t, local_t = expert_weight.T, local_choice.T
+    operands = (
+        group_choice.reshape(1, token_count), weight, weights_t, local_t,
+        tokens, cotangent, w_gate[0], w_up[0], w_down[0],
+    )
+    operands = [pltpu.with_memory_space_constraint(array, pltpu.HBM) for array in operands]
+    token_grad, gate_grad, first_grad, second_grad, third_grad = route(
+        *operands, group_count, lane_count, group_cap
+    )
+    group_grad, expert_grad, token_grad, first_grad, second_grad, third_grad = finish(
+        weight, weights_t, local_t, gate_grad, token_grad, first_grad, second_grad, third_grad
+    )
     return (
         token_grad,
-        group_grad,
-        expert_grad,
+        group_grad.reshape(token_count),
+        expert_grad.T,
         first_grad[None],
         second_grad[None],
         third_grad[None],

time: 95 us -> 73 us (0.77)
  local copies, waits for them, and re-layouts: 9.6 us -> 0.01 us
  Pallas kernels: 78.7 us -> 72.1 us
  other arithmetic: 5.66 us -> 0 us
    pallas_call x1, Pallas kernels: 78.7 us -> 68.7 us  [route(): pl.pallas_call(functools.partial(kernel, groups, lanes, cap, wide0, wide1...]
    unnamed x13 -> x6, local copies, waits for them, and re-layouts: 6.87 us -> 0.01 us
    pallas_call x0 -> x1, Pallas kernels: none -> 3.41 us  [finish(): pl.pallas_call(finish_kernel, out_shape=(like(weight), like(weights_t), l...]
    slice x2 -> x0, local copies, waits for them, and re-layouts: 2.73 us -> none  [the longest x1 1.88 us: shards(): token_grad = result[:, :piece]]
    reduce_sum x3 -> x0, other arithmetic: 2.52 us -> none  [the longest x1 1.44 us: shards(): jnp.sum(jnp.where(named, gate[:, :, None], 0), axis=1).astype(jnp.bfloat16)]
    convert_element_type x2 -> x0, other arithmetic: 1.4 us -> none  [the longest x1 0.71 us: shards(): (jnp.arange(row_count, dtype=jnp.int32)[:, None] == dest[None, :]).astype...]
    mul x1 -> x0, other arithmetic: 1.08 us -> none  [shards(): expert_grad = group_weight[:, None] * gate_grad]
where the time goes in v2:
time: 73 us; the launch traced here: 72.8 us
  Pallas kernels  72.1 us (99%)
    pallas_call x1, Pallas kernels, route(): pl.pallas_call(functools.partial(kernel, groups, lanes, cap, wide0, wide1...  68.7 us
    pallas_call x1, Pallas kernels, finish(): pl.pallas_call(finish_kernel, out_shape=(like(weight), like(weights_t), l...  3.41 us

profile of v2, /device:TPU:0, one launch (start us, length us, event | category | flops | bytes accessed | tf_op | source)
XLA Modules:
  0.0 72.8 jit_solution(3817522787457002915)
XLA Ops:
  0.6 0.0 copy-start
  0.6 0.0 copy-start.1
  0.7 0.0 copy-start.2
  0.7 68.7 %routed_backward.1 = (f32[128,1024]{1,0:T(8,128)S(1)}, f32[128,128]{1,0:T(8,128)S(1)}, f32[2048,256]{1,0:T(8,128)S(1)}, f32[2048,256]{1,0:T(8,128)S(1)}, f32[256,2048]{1,0:T(8,128)S(1)}) custom-call(s32[1,128]{1,0:T(1,128)} %bitcast.21, f32[1,128]{1,0:T(1,128)} %bitcast.16, f32[2,128]{1,0:T(2,128)} %bitcast.12, s32[2,128]{1,0:T(2,128)} %bitcast.14, ...), custom_call_target="tpu_custom_call" | custom-call | tf_op jit(solution)/shard_map/routed_backward/pallas_call | solution.py:463
  69.4 0.0 copy-done
  69.4 0.0 copy-done.1
  69.4 0.0 copy-done.2
  69.4 3.4 %write_results.1 = (f32[1,128]{1,0:T(1,128)}, f32[2,128]{1,0:T(2,128)}, f32[128,1024]{1,0:T(8,128)}, f32[2048,256]{1,0:T(8,128)}, f32[2048,256]{1,0:T(8,128)}, /*index=5*/f32[256,2048]{1,0:T(8,128)}) custom-call(f32[1,128]{1,0:T(1,128)S(1)} %bitcast.17, f32[2,128]{1,0:T(2,128)S(1)} %bitcast.13, s32[2,128]{1,0:T(2,128)S(1)} %bitcast.15, ...), custom_call_target="tpu_custom_call" | custom-call | tf_op jit(solution)/shard_map/write_results/pallas_call | solution.py:554
Async XLA Ops:
  0.6 68.8 %copy-start = (f32[128,2]{0,1:T(2,128)S(1)}, f32[128,2]{0,1:T(2,128)}, u32[]{:S(2)}) copy-start(f32[128,2]{0,1:T(2,128)} %param.12) | copy-start | bytes 3076
  0.6 68.8 %copy-start.1 = (s32[128,2]{0,1:T(2,128)S(1)}, s32[128,2]{0,1:T(2,128)}, u32[]{:S(2)}) copy-start(s32[128,2]{0,1:T(2,128)} %param.14) | copy-start | bytes 3076
  0.7 68.8 %copy-start.2 = (f32[128]{0:T(128)S(1)}, f32[128]{0:T(128)}, u32[]{:S(2)}) copy-start(f32[128]{0:T(128)} %param.11) | copy-start | bytes 1540

commit v3 on v2

--- a/solution.py
+++ b/solution.py
@@ -9,6 +9,8 @@
 
 EPG = 4
 LANES = 128
+PACKED = 16
+SENDS = 32
 VMEM_LIMIT = 36 * 1024 * 1024
 FINISH_LIMIT = 16 * 1024 * 1024
 
@@ -29,19 +31,20 @@
     return met
 
 
-def swapped(g, groups):
+def is_inner(g, groups):
     return 0 if groups & (groups - 1) else (g + g // 2) % 2
 
 
 class Copies:
     def __init__(self, send_sem, recv_sem):
         self.send_sem, self.recv_sem, self.count, self.made = send_sem, recv_sem, 0, []
-
-    def describe(self, src, dst, device, number):
+        self.kept = []
+
+    def describe(self, src, dst, device, number, slot):
         return pltpu.make_async_remote_copy(
             src_ref=src,
             dst_ref=dst,
-            send_sem=self.send_sem.at[number],
+            send_sem=self.send_sem.at[slot],
             recv_sem=self.recv_sem.at[number],
             device_id=device,
             device_id_type=MESH,
@@ -51,23 +54,32 @@
         self.count += count
         return self.count - count
 
-    def start(self, src, dst, device):
-        copy = self.describe(src, dst, device, self.reserve(1))
+    def start(self, src, dst, device, number=None):
+        slot = len(self.made) % SENDS
+        if len(self.made) >= SENDS:
+            self.made[len(self.made) - SENDS].wait_send()
+        number = self.reserve(1) if number is None else number
+        copy = self.describe(src, dst, device, number, slot)
         copy.start()
         self.made.append(copy)
         return copy
 
     def finish(self):
-        for copy in self.made:
+        for copy in self.kept + self.made[-SENDS:]:
             copy.wait_send()
+
+
+def whole_groups(groups, lanes):
+    return range(1, min(groups, 2)) if lanes == 2 else range(0)
 
 
 def copy_count(groups, lanes):
     far = lanes - 1
-    first = (groups - 1) * 3
-    spread = (groups - 1) * (2 + 4 * far) + 2 + 2 * far
-    inside = groups * 7
-    back = groups * (4 + 2 * far) + groups - 1
+    whole = len(whole_groups(groups, lanes))
+    first = (groups - 1) * 3 + whole * 2 * far
+    spread = (groups - 1 - whole) * (2 + 4 * far) + (1 + whole) * (2 + 2 * far)
+    inside = groups * 4
+    back = groups * (6 + 3 * far) + 2 * (groups - 1)
     return first + spread + inside + back
 
 
@@ -83,41 +95,71 @@
 
 
 def plan(groups):
-    steps = [("own", 0), ("relay_t", 0)]
-    if groups > 1:
-        steps += [("arrive_t", 1), ("relay_c", 0), ("arrive_c", 1), ("relay_t", 1), ("relay_c", 1)]
-    else:
-        steps += [("relay_c", 0), ("inside_t", 0), ("inside_c", 0), ("compute", 0)]
-    for d in range(1, groups):
-        more = d + 1 < groups
-        if more:
-            steps.append(("arrive_t", d + 1))
-        if d == 1:
-            steps += [("inside_t", 0), ("inside_c", 0), ("compute", 0)]
-        steps.append(("inside_t", d))
-        if more:
-            steps.append(("arrive_c", d + 1))
-        steps.append(("inside_c", d))
-        if more:
-            steps += [("relay_t", d + 1), ("relay_c", d + 1)]
-        steps.append(("compute", d))
-        if d > 1:
-            steps.append(("sum_cores", d - 1))
-    order = list(range(1, groups)) + [0]
-    stage = {d: 1 for d in range(1, groups - 1)}
-    waiting = [d for d in order if d not in stage]
-    while stage or waiting:
-        if waiting:
-            d = waiting.pop(0)
-            steps.append(("sum_cores", d))
-            stage[d] = 1
-        steps.append(("weights", 0))
-        for d in [d for d in order if stage.get(d) == 2][:1]:
-            steps.append(("last_sum", d))
-            del stage[d]
-        for d in [d for d in order if stage.get(d) == 1][:1]:
-            steps.append(("middle_sum", d))
-            stage[d] = 2
+    steps = []
+
+    def put(names, d):
+        for name in names.split():
+            if (0 <= d < groups or name == "weights") and (name, d) not in steps and (d or not name.startswith("arrive")):
+                steps.append((name, d))
+
+    put("own relay_t", 0)
+    put("arrive_t", 1)
+    put("next_t relay_c", 0)
+    put("arrive_c relay_t", 1)
+    put("next_c", 0)
+    put("relay_c", 1)
+    put("inside_t inside_c", 0)
+    put("arrive_t", 2)
+    put("rest_t compute", 0)
+    put("inside_t inside_c", 1)
+    put("arrive_c", 2)
+    put("rest_c", 0)
+    put("relay_t", 2)
+    put("inside_z", 1)
+    put("relay_c", 2)
+    for d in range(3, groups):
+        put("arrive_t arrive_c", d)
+        put("compute", d - 2)
+        put("inside_t inside_c", d - 1)
+        put("relay_t relay_c", d)
+        put("sum_cores", d - 2)
+        put("sum_cores", 0)
+        put("compute", d - 1)
+        if d < groups - 1:
+            put("middle_sum last_sum", d - 2)
+    last = groups - 1
+    before = last - 1 if last > 2 else 0
+    put("compute", 1)
+    put("inside_t", last)
+    if before:
+        put("sum_cores", before)
+    put("inside_c", last)
+    if before:
+        put("middle_sum", before - 1)
+        put("middle_sum", 0)
+    put("compute", last)
+    if before:
+        put("last_sum", before - 1)
+        put("middle_sum", before)
+    if last > 0:
+        put("sum_cores", last)
+    put("weights", 0)
+    if before:
+        put("last_sum", 0)
+    if before:
+        put("last_sum", before)
+    put("weights", 1)
+    if last > 0:
+        put("middle_sum", last)
+    put("sum_cores", 0)
+    if last == 2:
+        put("sum_cores middle_sum last_sum", 1)
+    put("weights", 2)
+    if last > 0:
+        put("last_sum", last)
+    put("middle_sum", 0)
+    put("weights", 3)
+    put("last_sum", 0)
     return steps
 
 
@@ -125,9 +167,9 @@
     groups, lanes, cap, wide0, wide1,
     choice_in, weight_in, weights_in, local_in, tokens_in, cotangent_in, w_gate, w_up, w_down,
     token_grad, gate_grad, grad_first, grad_second, grad_third,
-    choice, weight, weights_t, local_t, tokens, cotangent, pick, out_t, out_c, out_g, tok, cot, gate, first, second, third,
+    choice, weight, weights_t, local_t, tokens, cotangent, pick, out_t, out_c, out_g, all_t, all_c, tok, cot, gate, first, second, third,
     gg, gu, wt, wt_t, part_a, part_b, rc_a, rc_b, s1_a, s1_b, rx_a, rl_a, rl_b, s2_a, s2_b, rx_b,
-    done, ret, send, recv, loc,
+    done, ret, part_g, rc_g, s1_g, rx_g, s2_g, rl_g, done_g, ret_g, send, recv, loc,
 ):
     g, e, y = lax.axis_index("g"), lax.axis_index("e"), lax.axis_index("tp")
     x, c = e // 2, e % 2
@@ -190,33 +232,87 @@
     out_t[...] = spread_rows(one_hot, tokens[:, columns]).reshape(groups, cap, piece)
     loads[5].wait()
     out_c[...] = spread_rows(one_hot, cotangent[:, columns]).reshape(groups, cap, piece)
+    whole = whole_groups(groups, lanes)
     pl.semaphore_wait(barrier, len(met))
 
     copies = Copies(send, recv)
     state = [dict() for _ in range(groups)]
     base = copies.reserve(3 * (groups - 1))
-    flip = swapped(g, groups)
 
     def cross(d, target):
         there = (target, e, y)
         number = base + 3 * (d - 1)
         return [
-            copies.describe(out_t.at[target], tok.at[y, d, 0], there, number),
-            copies.describe(out_g.at[target], gate.at[d, 0], there, number + 1),
-            copies.describe(out_c.at[target], cot.at[y, d, 0], there, number + 2),
+            copies.describe(out_t.at[target], tok.at[y, d, 0], there, number, SENDS + number),
+            copies.describe(out_g.at[target], gate.at[d, 0], there, number + 1, SENDS + number + 1),
+            copies.describe(out_c.at[target], cot.at[y, d, 0], there, number + 2, SENDS + number + 2),
         ]
 
-    for k in range(1, groups):
-        d, target = k, partner(g, k, groups, -1)
-        if k > 1 and not isinstance(flip, int):
-            d = k + flip * (1 - 2 * (k % 2))
-            target = target + flip * (1 - 2 * (target % 2))
-        for copy in cross(d, target):
-            copy.start()
+    def send(ds, kinds):
+        for d in ds:
+            for kind in kinds:
+                cross(d, partner(g, d, groups, -1))[kind].start()
+
+    inner = is_inner(g, groups)
+    far_first = groups > 3 and not isinstance(inner, int)
+    send(range(1, min(groups, 2)), (0, 1, 2))
+    if far_first:
+        pl.when(inner == 1)(lambda: send([3], (0, 1, 2)))
+    for d in whole:
+        mine = pick[partner(g, d, groups, -1)]
+        for lane in range(lanes):
+            cols = slice(lane * piece, (lane + 1) * piece)
+            all_t[d, lane] = spread_rows(mine, tokens[:, cols])
+            all_c[d, lane] = spread_rows(mine, cotangent[:, cols])
+
+    def send_whole(source, target, name):
+        for d in whole:
+            there = (partner(g, d, groups, -1), e, y)
+            state[d][name] = [
+                copies.start(source.at[d, lane], target.at[lane, d, 0], there) for lane in ahead
+            ]
+
+    def next_t(_):
+        send(range(2, min(groups, 3)), (0, 1))
+        send_whole(all_t, tok, "zat")
+
+    def next_c(_):
+        send(range(2, min(groups, 3)), (2,))
+        send_whole(all_c, cot, "zac")
+
+    def rest(kinds):
+        if far_first:
+            pl.when(inner == 0)(lambda: send([3], kinds))
+        send(range(4 if far_first else 3, groups), kinds)
+
+    def rest_t(_):
+        rest((0, 1))
+
+    def rest_c(_):
+        rest((2,))
+
     for d in range(1, groups):
         arriving = cross(d, partner(g, d, groups, -1))
-        copies.made += arriving
+        copies.kept += arriving
         state[d]["zt"], state[d]["zg"], state[d]["zc"] = arriving
+
+    inner_base = copies.reserve(3 * groups)
+
+    def to_core(d, kind, slot):
+        ref = (tok, gate, cot)[kind]
+        if kind == 1:
+            src, dst = gate.at[d, slot], gate.at[d, slot + 2]
+        else:
+            src, dst = ref.at[:, d, slot], ref.at[:, d, slot + 2]
+        copies.start(src, dst, ec, inner_base + 3 * d + kind)
+
+    def wait_core(d):
+        for kind, ref in enumerate((tok, gate, cot)):
+            if kind == 1:
+                src, dst = gate.at[d, pl.ds(0, 2)], gate.at[d, pl.ds(2, 2)]
+            else:
+                src, dst = ref.at[:, d, pl.ds(0, 2)], ref.at[:, d, pl.ds(2, 2)]
+            copies.describe(src, dst, ec, inner_base + 3 * d + kind, 0).wait_recv()
 
     def own(_):
         s = state[0]
@@ -229,41 +325,40 @@
             tok[lane, 0, 0] = spread_rows(mine, tokens[:, cols])
             cot[lane, 0, 0] = spread_rows(mine, cotangent[:, cols])
         gate[0, 0] = out_g[g]
-        s["core"] = [
-            copies.start(out_g.at[g], gate.at[0, 2], ec),
-            copies.start(tok.at[:, 0, 0], tok.at[:, 0, 2], ec),
-            copies.start(cot.at[:, 0, 0], cot.at[:, 0, 2], ec),
-        ]
+        for kind in (1, 0, 2):
+            to_core(0, kind, 0)
 
     def arrive_t(d):
         s = state[d]
         s["zt"].wait_recv()
         mine = tok.at[y, d, 0]
-        s["tl"] = [copies.start(mine, mine, device) for device in others]
+        if d not in whole:
+            s["tl"] = [copies.start(mine, mine, device) for device in others]
         s["tx"] = [copies.start(mine, tok.at[y, d, 1], ex)]
         s["zg"].wait_recv()
         s["gx"] = copies.start(gate.at[d, 0], gate.at[d, 1], ex)
-        s["core"] = [copies.start(gate.at[d, 0], gate.at[d, 2], ec)]
+        to_core(d, 1, 0)
 
     def arrive_c(d):
         s = state[d]
         s["zc"].wait_recv()
         mine = cot.at[y, d, 0]
         s["cx"] = copies.start(mine, cot.at[y, d, 1], ex)
-        s["cl"] = [copies.start(mine, mine, device) for device in others]
+        if d not in whole:
+            s["cl"] = [copies.start(mine, mine, device) for device in others]
 
     def relay_t(d):
         s = state[d]
-        if d == 0:
+        if d == 0 or d in whole:
             s["tx"][0].wait_recv()
-            theirs = tok.at[y, 0, 1]
+            theirs = tok.at[y, d, 1]
             s["txl"] = [copies.start(theirs, theirs, device) for device in others]
         else:
             for i, copy in enumerate(s["tl"]):
                 copy.wait_recv()
                 theirs = tok.at[behind[i], d, 0]
                 s["tx"].append(copies.start(theirs, tok.at[behind[i], d, 1], ex))
-            s["core"].append(copies.start(tok.at[:, d, 0], tok.at[:, d, 2], ec))
+            to_core(d, 0, 0)
 
     def relay_c(d):
         s = state[d]
@@ -271,26 +366,36 @@
         theirs = cot.at[y, d, 1]
         s["cxl"] = [copies.start(theirs, theirs, device) for device in others]
 
+    def inside_z(d):
+        s = state[d]
+        if d in whole:
+            for copy in s["zat"]:
+                copy.wait_recv()
+            to_core(d, 0, 0)
+            for copy in s["zac"]:
+                copy.wait_recv()
+            to_core(d, 2, 0)
+
     def inside_t(d):
         s = state[d]
-        if d == 0:
+        if d == 0 or d in whole:
             for copy in s["txl"]:
                 copy.wait_recv()
         else:
             for copy in s["cl"]:
                 copy.wait_recv()
-            s["core"].append(copies.start(cot.at[:, d, 0], cot.at[:, d, 2], ec))
+            to_core(d, 2, 0)
             for copy in s["tx"]:
                 copy.wait_recv()
-        s["core"].append(copies.start(tok.at[:, d, 1], tok.at[:, d, 3], ec))
+        to_core(d, 0, 1)
 
     def inside_c(d):
         s = state[d]
         s["gx"].wait_recv()
-        s["core"].append(copies.start(gate.at[d, 1], gate.at[d, 3], ec))
+        to_core(d, 1, 1)
         for copy in s["cxl"]:
             copy.wait_recv()
-        s["core"].append(copies.start(cot.at[:, d, 1], cot.at[:, d, 3], ec))
+        to_core(d, 2, 1)
 
     loaded = []
 
@@ -300,8 +405,7 @@
             for load in loads[6:]:
                 load.wait()
             loaded.append(True)
-        for copy in s["core"]:
-            copy.wait_recv()
+        wait_core(d)
         pre_gate = pre_up = back = None
         for lane in range(lanes):
             cols = slice(lane * piece, (lane + 1) * piece)
@@ -331,34 +435,62 @@
         wt[at, :] = (gate_float * hidden).astype(jnp.bfloat16)
         gate_out = jnp.where(own_col, gate_part, 0.0).astype(jnp.bfloat16)
 
-        def rows_back(lo, hi):
+        packed_width = part_g.shape[3]
+        blocks = gate_out.reshape(EPG, cap, LANES)
+        if packed_width > cap:
+            filler = jnp.zeros((EPG, packed_width - cap, LANES), jnp.bfloat16)
+            blocks = jnp.concatenate([blocks, filler], axis=1)
+        chooser = jnp.where(iota((PACKED, LANES), 0) == iota((PACKED, LANES), 1), 1.0, 0.0)
+        packed = lax.dot_general(
+            chooser.astype(jnp.bfloat16),
+            blocks.reshape(EPG * packed_width, LANES),
+            CONTRACT_COLS,
+            preferred_element_type=jnp.float32,
+        ).astype(jnp.bfloat16)
+        for slot in range(EPG):
+            part_g[d, slot] = packed[:, slot * packed_width : (slot + 1) * packed_width]
+        s["pg"] = copies.start(part_g.at[d, pl.ds(2, 2)], rc_g.at[d], ec)
+        shares = 2 if d == groups - 1 else 1
+        kept = EPG // shares
+
+        def rows_back(lo, hi, half):
+            part = slice(half * rows // shares, (half + 1) * rows // shares)
             total = lax.dot_general(
-                grad_gate, first[lo:hi, :], CONTRACT_COLS, preferred_element_type=jnp.float32
+                grad_gate[part], first[lo:hi, :], CONTRACT_COLS, preferred_element_type=jnp.float32
             ) + lax.dot_general(
-                grad_up, second[lo:hi, :], CONTRACT_COLS, preferred_element_type=jnp.float32
+                grad_up[part], second[lo:hi, :], CONTRACT_COLS, preferred_element_type=jnp.float32
             )
-            return total.astype(jnp.bfloat16).reshape(EPG, cap, hi - lo)
-
-        for lane in range(lanes):
-            lo = lane * piece
-            part_a[d, lane] = rows_back(lo, lo + wide0)
-            if wide0 < piece:
-                part_b[d, lane, :, :, : piece - wide0] = rows_back(lo + wide0, lo + piece)
-            part_b[d, lane, :, :, piece - wide0 :] = gate_out.reshape(EPG, cap, LANES)
-        s["pa"] = copies.start(part_a.at[d, :, pl.ds(2, 2)], rc_a.at[d], ec)
-        s["pb"] = copies.start(part_b.at[d, :, pl.ds(2, 2)], rc_b.at[d], ec)
+            return total.astype(jnp.bfloat16).reshape(kept, cap, hi - lo)
+
+        for half in reversed(range(shares)):
+            slots = slice(half * kept, (half + 1) * kept)
+            for lane in range(lanes):
+                lo = lane * piece
+                part_a[d, lane, slots] = rows_back(lo, lo + wide0, half)
+            if half == shares - 1:
+                s["pa"] = copies.start(part_a.at[d, :, pl.ds(2, 2)], rc_a.at[d], ec)
+            for lane in range(lanes):
+                lo = lane * piece
+                if wide1:
+                    part_b[d, lane, slots] = rows_back(lo + wide0, lo + piece, half)
+            if half == shares - 1 and wide1:
+                s["pb"] = copies.start(part_b.at[d, :, pl.ds(2, 2)], rc_b.at[d], ec)
 
     def sum_cores(d):
         s = state[d]
         s["pa"].wait_recv()
         s1_a[d] = add(part_a[d, :, 0:2], rc_a[d])
         s["x0"] = copies.start(s1_a.at[d, :, 1], rx_a.at[d], ex)
-        s["pb"].wait_recv()
-        s1_b[d] = add(part_b[d, :, 0:2], rc_b[d])
-        s["l1"] = [
-            copies.start(s1_b.at[d, lane], rl_b.at[d, i], (g, e, lane))
-            for i, lane in enumerate(ahead)
-        ]
+        s["pg"].wait_recv()
+        s1_g[d] = add(part_g[d, 0:2], rc_g[d])
+        s["xg"] = copies.start(s1_g.at[d, 1], rx_g.at[d], ex)
+        if wide1:
+            s["pb"].wait_recv()
+            s1_b[d] = add(part_b[d, :, 0:2], rc_b[d])
+            s["l1"] = [
+                copies.start(s1_b.at[d, lane], rl_b.at[d, i], (g, e, lane))
+                for i, lane in enumerate(ahead)
+            ]
 
     def middle_sum(d):
         s = state[d]
@@ -368,26 +500,35 @@
             copies.start(s2_a.at[d, lane], rl_a.at[d, i], (g, e, lane))
             for i, lane in enumerate(ahead)
         ]
-        for copy in s["l1"]:
-            copy.wait_recv()
-        s2_b[d] = add(s1_b[d, y], *[rl_b[d, i] for i in range(lanes - 1)])
-        s["x1"] = copies.start(s2_b.at[d, 1], rx_b.at[d], ex)
+        s["xg"].wait_recv()
+        s2_g[d] = add(s1_g[d, 0], rx_g[d])
+        s["lg"] = [
+            copies.start(s2_g.at[d], rl_g.at[d, i], (g, e, lane)) for i, lane in enumerate(ahead)
+        ]
+        if wide1:
+            for copy in s["l1"]:
+                copy.wait_recv()
+            s2_b[d] = add(s1_b[d, y], *[rl_b[d, i] for i in range(lanes - 1)])
+            s["x1"] = copies.start(s2_b.at[d, 1], rx_b.at[d], ex)
 
     def last_sum(d):
         s = state[d]
+        rows_at, gates_at, at = (ret, ret_g, g) if d == 0 else (done, done_g, d)
         for copy in s["l0"]:
             copy.wait_recv()
-        head = add(s2_a[d, y], *[rl_a[d, i] for i in range(lanes - 1)])
-        s["x1"].wait_recv()
-        tail = add(s2_b[d, 0], rx_b[d])
-        if d == 0:
-            ret[g, :, :wide0] = head
-            ret[g, :, wide0:] = tail
-        else:
-            done[d, :, :wide0] = head
-            done[d, :, wide0:] = tail
+        rows_at[at, :, :wide0] = add(s2_a[d, y], *[rl_a[d, i] for i in range(lanes - 1)])
+        for copy in s["lg"]:
+            copy.wait_recv()
+        gates_at[at] = add(s2_g[d], *[rl_g[d, i] for i in range(lanes - 1)])
+        if wide1:
+            s["x1"].wait_recv()
+            rows_at[at, :, wide0:] = add(s2_b[d, 0], rx_b[d])
+        if d:
             there = (partner(g, d, groups, 1), e, y)
-            s["z"] = copies.start(done.at[d], ret.at[g], there)
+            s["z"] = [
+                copies.start(done.at[d], ret.at[g], there),
+                copies.start(done_g.at[d], ret_g.at[g], there),
+            ]
 
     tile = min(2 * LANES, piece)
     per = piece // tile
@@ -423,32 +564,37 @@
 
     phases = {
         "own": own, "arrive_t": arrive_t, "arrive_c": arrive_c, "relay_t": relay_t,
-        "relay_c": relay_c, "inside_t": inside_t, "inside_c": inside_c, "compute": compute,
+        "relay_c": relay_c, "inside_t": inside_t, "inside_z": inside_z, "inside_c": inside_c, "compute": compute,
         "sum_cores": sum_cores, "middle_sum": middle_sum, "last_sum": last_sum,
-        "weights": weights,
+        "weights": weights, "next_t": next_t, "next_c": next_c, "rest_t": rest_t, "rest_c": rest_c,
     }
     for name, d in steps:
         with jax.named_scope(f"{name}_{d}"):
             phases[name](d)
     with jax.named_scope("gather"):
         for d in range(1, groups):
-            state[d]["z"].wait_recv()
-        back = ret[...].reshape(groups * cap, wide0 + wide1)
+            for copy in state[d]["z"]:
+                copy.wait_recv()
         token_grad[...] = lax.dot_general(
-            one_hot, back[:, :piece], CONTRACT_ROWS, preferred_element_type=jnp.float32
+            one_hot, ret[...].reshape(groups * cap, piece), CONTRACT_ROWS,
+            preferred_element_type=jnp.float32,
         )
-        gate_grad[...] = lax.dot_general(
-            back[:, piece:], one_hot, CONTRACT_ROWS, preferred_element_type=jnp.float32
-        )
-    copies.finish()
+        total = dot(ret_g[0, :, :cap], pick[0])
+        for group in range(1, groups):
+            total = total + dot(ret_g[group, :, :cap], pick[group])
+        gate_grad[...] = total
+    with jax.named_scope("finish"):
+        copies.finish()
 
 
 def route(choice, weight, weights_t, local_t, tokens, cotangent, w_gate, w_up, w_down, groups, lanes, cap):
     token_count, feature_count = tokens.shape
     hidden_count = w_gate.shape[1]
     piece = feature_count // lanes
-    wide1 = (piece + LANES) // (2 * LANES) * LANES
-    wide0 = piece + LANES - wide1
+    wide1 = piece // (2 * LANES) * LANES
+    wide0 = piece - wide1
+    tail = max(wide1, LANES)
+    packed = -(-cap // LANES) * LANES
     rows = EPG * cap
     far = max(lanes - 1, 1)
     count = copy_count(groups, lanes)
@@ -464,7 +610,7 @@
         functools.partial(kernel, groups, lanes, cap, wide0, wide1),
         out_shape=(
             grad(token_count, piece),
-            grad(LANES, token_count),
+            grad(PACKED, token_count),
             grad(feature_count, hidden_count),
             grad(feature_count, hidden_count),
             grad(hidden_count, feature_count),
@@ -482,6 +628,8 @@
             buffer(groups, cap, piece),
             buffer(groups, cap, piece),
             buffer(groups, cap, LANES),
+            buffer(2, lanes, cap, piece),
+            buffer(2, lanes, cap, piece),
             buffer(lanes, groups, EPG, cap, piece),
             buffer(lanes, groups, EPG, cap, piece),
             buffer(groups, EPG, cap, LANES),
@@ -493,20 +641,28 @@
             buffer(groups * rows, hidden_count),
             buffer(hidden_count, groups * rows),
             buffer(groups, lanes, EPG, cap, wide0),
-            buffer(groups, lanes, EPG, cap, wide1),
+            buffer(groups, lanes, EPG, cap, tail),
             buffer(groups, lanes, 2, cap, wide0),
-            buffer(groups, lanes, 2, cap, wide1),
+            buffer(groups, lanes, 2, cap, tail),
             buffer(groups, lanes, 2, cap, wide0),
-            buffer(groups, lanes, 2, cap, wide1),
+            buffer(groups, lanes, 2, cap, tail),
             buffer(groups, lanes, cap, wide0),
             buffer(groups, far, cap, wide0),
-            buffer(groups, far, 2, cap, wide1),
+            buffer(groups, far, 2, cap, tail),
             buffer(groups, lanes, cap, wide0),
-            buffer(groups, 2, cap, wide1),
-            buffer(groups, cap, wide1),
-            buffer(groups, cap, wide0 + wide1),
-            buffer(groups, cap, wide0 + wide1),
-            pltpu.SemaphoreType.DMA((count,)),
+            buffer(groups, 2, cap, tail),
+            buffer(groups, cap, tail),
+            buffer(groups, cap, piece),
+            buffer(groups, cap, piece),
+            buffer(groups, EPG, PACKED, packed),
+            buffer(groups, 2, PACKED, packed),
+            buffer(groups, 2, PACKED, packed),
+            buffer(groups, PACKED, packed),
+            buffer(groups, PACKED, packed),
+            buffer(groups, far, PACKED, packed),
+            buffer(groups, PACKED, packed),
+            buffer(groups, PACKED, packed),
+            pltpu.SemaphoreType.DMA((SENDS + 3 * max(groups - 1, 1),)),
             pltpu.SemaphoreType.DMA((count,)),
             pltpu.SemaphoreType.DMA((9,)),
         ],

time: 73 us -> 62 us (0.85)
  Pallas kernels: 72.1 us -> 61.2 us
    pallas_call x1, Pallas kernels: 68.7 us -> 57.8 us  [route(): pl.pallas_call(functools.partial(kernel, groups, lanes, cap, wide0, wide1...]
where the time goes in v3:
time: 62 us; the launch traced here: 61.9 us
  Pallas kernels  61.2 us (99%)
  between operations  0.69 us (1%)
    pallas_call x1, Pallas kernels, route(): pl.pallas_call(functools.partial(kernel, groups, lanes, cap, wide0, wide1...  57.8 us
    pallas_call x1, Pallas kernels, finish(): pl.pallas_call(finish_kernel, out_shape=(like(weight), like(weights_t), l...  3.41 us

profile of v3, /device:TPU:0, one launch (start us, length us, event | category | flops | bytes accessed | tf_op | source)
XLA Modules:
  0.0 61.9 jit_solution(10804075118226575953)
XLA Ops:
  0.6 0.0 copy-start
  0.6 0.0 copy-start.1
  0.7 0.0 copy-start.2
  0.7 57.8 %routed_backward.1 = (f32[128,1024]{1,0:T(8,128)S(1)}, f32[16,128]{1,0:T(8,128)S(1)}, f32[2048,256]{1,0:T(8,128)S(1)}, f32[2048,256]{1,0:T(8,128)S(1)}, f32[256,2048]{1,0:T(8,128)S(1)}) custom-call(s32[1,128]{1,0:T(1,128)} %bitcast.21, f32[1,128]{1,0:T(1,128)} %bitcast.16, f32[2,128]{1,0:T(2,128)} %bitcast.12, s32[2,128]{1,0:T(2,128)} %bitcast.14, ...), custom_call_target="tpu_custom_call" | custom-call | tf_op jit(solution)/shard_map/routed_backward/pallas_call | solution.py:609
  58.4 0.0 copy-done
  58.4 0.0 copy-done.1
  58.4 0.0 copy-done.2
  58.5 3.4 %write_results.1 = (f32[1,128]{1,0:T(1,128)}, f32[2,128]{1,0:T(2,128)}, f32[128,1024]{1,0:T(8,128)}, f32[2048,256]{1,0:T(8,128)}, f32[2048,256]{1,0:T(8,128)}, /*index=5*/f32[256,2048]{1,0:T(8,128)}) custom-call(f32[1,128]{1,0:T(1,128)S(1)} %bitcast.17, f32[2,128]{1,0:T(2,128)S(1)} %bitcast.13, s32[2,128]{1,0:T(2,128)S(1)} %bitcast.15, ...), custom_call_target="tpu_custom_call" | custom-call | tf_op jit(solution)/shard_map/write_results/pallas_call | solution.py:710
Async XLA Ops:
  0.6 57.8 %copy-start = (f32[128,2]{0,1:T(2,128)S(1)}, f32[128,2]{0,1:T(2,128)}, u32[]{:S(2)}) copy-start(f32[128,2]{0,1:T(2,128)} %param.12) | copy-start | bytes 3076
  0.6 57.8 %copy-start.1 = (s32[128,2]{0,1:T(2,128)S(1)}, s32[128,2]{0,1:T(2,128)}, u32[]{:S(2)}) copy-start(s32[128,2]{0,1:T(2,128)} %param.14) | copy-start | bytes 3076
  0.7 57.8 %copy-start.2 = (f32[128]{0:T(128)S(1)}, f32[128]{0:T(128)}, u32[]{:S(2)}) copy-start(f32[128]{0:T(128)} %param.11) | copy-start | bytes 1540

commit v4 on v3

--- a/solution.py
+++ b/solution.py
@@ -11,6 +11,7 @@
 LANES = 128
 PACKED = 16
 SENDS = 32
+PARTS = 4
 VMEM_LIMIT = 36 * 1024 * 1024
 FINISH_LIMIT = 16 * 1024 * 1024
 
@@ -79,7 +80,7 @@
     first = (groups - 1) * 3 + whole * 2 * far
     spread = (groups - 1 - whole) * (2 + 4 * far) + (1 + whole) * (2 + 2 * far)
     inside = groups * 4
-    back = groups * (6 + 3 * far) + 2 * (groups - 1)
+    back = groups * (6 + 3 * far) + 3 * (groups - 1)
     return first + spread + inside + back
 
 
@@ -102,9 +103,9 @@
             if (0 <= d < groups or name == "weights") and (name, d) not in steps and (d or not name.startswith("arrive")):
                 steps.append((name, d))
 
-    put("own relay_t", 0)
+    put("own next_t relay_t", 0)
     put("arrive_t", 1)
-    put("next_t relay_c", 0)
+    put("relay_c", 0)
     put("arrive_c relay_t", 1)
     put("next_c", 0)
     put("relay_c", 1)
@@ -116,6 +117,7 @@
     put("rest_c", 0)
     put("relay_t", 2)
     put("inside_z", 1)
+    put("arrive_t", 3)
     put("relay_c", 2)
     for d in range(3, groups):
         put("arrive_t arrive_c", d)
@@ -134,18 +136,19 @@
     if before:
         put("sum_cores", before)
     put("inside_c", last)
+    if last > 1:
+        put("compute_t", last)
     if before:
         put("middle_sum", before - 1)
-        put("middle_sum", 0)
     put("compute", last)
     if before:
-        put("last_sum", before - 1)
         put("middle_sum", before)
     if last > 0:
         put("sum_cores", last)
     put("weights", 0)
     if before:
-        put("last_sum", 0)
+        put("last_sum", before - 1)
+        put("middle_sum", 0)
     if before:
         put("last_sum", before)
     put("weights", 1)
@@ -157,9 +160,8 @@
     put("weights", 2)
     if last > 0:
         put("last_sum", last)
-    put("middle_sum", 0)
+    put("middle_sum last_sum", 0)
     put("weights", 3)
-    put("last_sum", 0)
     return steps
 
 
@@ -168,7 +170,7 @@
     choice_in, weight_in, weights_in, local_in, tokens_in, cotangent_in, w_gate, w_up, w_down,
     token_grad, gate_grad, grad_first, grad_second, grad_third,
     choice, weight, weights_t, local_t, tokens, cotangent, pick, out_t, out_c, out_g, all_t, all_c, tok, cot, gate, first, second, third,
-    gg, gu, wt, wt_t, part_a, part_b, rc_a, rc_b, s1_a, s1_b, rx_a, rl_a, rl_b, s2_a, s2_b, rx_b,
+    pre, gg, gu, wt, wt_t, part_a, part_b, rc_a, rc_b, s1_a, s1_b, rx_a, rl_a, rl_b, s2_a, s2_b, rx_b,
     done, ret, part_g, rc_g, s1_g, rx_g, s2_g, rl_g, done_g, ret_g, send, recv, loc,
 ):
     g, e, y = lax.axis_index("g"), lax.axis_index("e"), lax.axis_index("tp")
@@ -192,7 +194,7 @@
             )
         )
     ]
-    for load in loads:
+    for load in loads[:6]:
         load.start()
     barrier = pltpu.get_barrier_semaphore()
     met = [(lax.rem(g + d, groups), e, y) for d in range(1, groups)] + others + [ex, ec]
@@ -219,15 +221,22 @@
     one_hot = jnp.where(iota((groups * cap, token_count), 0) == dest, 1.0, 0.0).astype(jnp.bfloat16)
     pick[...] = one_hot.reshape(groups, cap, token_count)
     gates = (weight[...] * weights_t[...]).astype(jnp.bfloat16).astype(jnp.float32)
-    gate_rows = jnp.zeros((LANES, token_count), jnp.float32)
+    gate_rows = jnp.zeros((PACKED, token_count), jnp.float32)
     for k in range(local_t.shape[0]):
-        hit = iota((LANES, token_count), 0) == local_t[k : k + 1, :]
+        hit = iota((PACKED, token_count), 0) == local_t[k : k + 1, :]
         gate_rows = gate_rows + jnp.where(hit, gates[k : k + 1, :], 0.0)
     columns = pl.ds(pl.multiple_of(y * piece, LANES), piece)
+    packed_width = out_g.shape[2]
+    wide_dest = chosen * packed_width + rank
+    wide_hot = iota((groups * packed_width, token_count), 0) == wide_dest
     blocks = lax.dot_general(
-        one_hot, gate_rows.astype(jnp.bfloat16), CONTRACT_COLS, preferred_element_type=jnp.float32
-    )
-    out_g[...] = blocks.astype(jnp.bfloat16).reshape(groups, cap, LANES)
+        gate_rows.astype(jnp.bfloat16),
+        jnp.where(wide_hot, 1.0, 0.0).astype(jnp.bfloat16),
+        CONTRACT_COLS,
+        preferred_element_type=jnp.float32,
+    ).astype(jnp.bfloat16)
+    for group in range(groups):
+        out_g[group] = blocks[:, group * packed_width : (group + 1) * packed_width]
     loads[4].wait()
     out_t[...] = spread_rows(one_hot, tokens[:, columns]).reshape(groups, cap, piece)
     loads[5].wait()
@@ -258,12 +267,16 @@
     send(range(1, min(groups, 2)), (0, 1, 2))
     if far_first:
         pl.when(inner == 1)(lambda: send([3], (0, 1, 2)))
-    for d in whole:
-        mine = pick[partner(g, d, groups, -1)]
-        for lane in range(lanes):
-            cols = slice(lane * piece, (lane + 1) * piece)
-            all_t[d, lane] = spread_rows(mine, tokens[:, cols])
-            all_c[d, lane] = spread_rows(mine, cotangent[:, cols])
+    for load in loads[6:]:
+        load.start()
+
+    def fill_whole():
+        for d in whole:
+            mine = pick[partner(g, d, groups, -1)]
+            for lane in ahead:
+                cols = pl.ds(pl.multiple_of(lane * piece, LANES), piece)
+                all_t[d, lane] = spread_rows(mine, tokens[:, cols])
+                all_c[d, lane] = spread_rows(mine, cotangent[:, cols])
 
     def send_whole(source, target, name):
         for d in whole:
@@ -306,8 +319,9 @@
             src, dst = ref.at[:, d, slot], ref.at[:, d, slot + 2]
         copies.start(src, dst, ec, inner_base + 3 * d + kind)
 
-    def wait_core(d):
-        for kind, ref in enumerate((tok, gate, cot)):
+    def wait_core(d, kinds):
+        for kind in kinds:
+            ref = (tok, gate, cot)[kind]
             if kind == 1:
                 src, dst = gate.at[d, pl.ds(0, 2)], gate.at[d, pl.ds(2, 2)]
             else:
@@ -327,6 +341,7 @@
         gate[0, 0] = out_g[g]
         for kind in (1, 0, 2):
             to_core(0, kind, 0)
+        fill_whole()
 
     def arrive_t(d):
         s = state[d]
@@ -399,29 +414,48 @@
 
     loaded = []
 
-    def compute(d):
-        s = state[d]
+    begun = set()
+
+    def compute_t(d):
+        begun.add(d)
         if not loaded:
             for load in loads[6:]:
                 load.wait()
             loaded.append(True)
-        wait_core(d)
-        pre_gate = pre_up = back = None
+        wait_core(d, (0,))
+        for half, weights_in in enumerate((first, second)):
+            total = None
+            for lane in range(lanes):
+                cols = slice(lane * piece, (lane + 1) * piece)
+                term = dot(tok[lane, d].reshape(rows, piece), weights_in[cols, :])
+                total = term if total is None else total + term
+            pre[half] = total
+
+    def compute(d):
+        s = state[d]
+        if d not in begun:
+            compute_t(d)
+        wait_core(d, (1, 2))
+        back = None
         for lane in range(lanes):
             cols = slice(lane * piece, (lane + 1) * piece)
-            rows_t = tok[lane, d].reshape(rows, piece)
-            rows_c = cot[lane, d].reshape(rows, piece)
-            one = dot(rows_t, first[cols, :])
-            two = dot(rows_t, second[cols, :])
-            three = lax.dot_general(
-                rows_c, third[:, cols], CONTRACT_COLS, preferred_element_type=jnp.float32
+            term = lax.dot_general(
+                cot[lane, d].reshape(rows, piece), third[:, cols], CONTRACT_COLS,
+                preferred_element_type=jnp.float32,
             )
-            pre_gate = one if lane == 0 else pre_gate + one
-            pre_up = two if lane == 0 else pre_up + two
-            back = three if lane == 0 else back + three
+            back = term if back is None else back + term
+        pre_gate, pre_up = pre[0], pre[1]
         own_col = iota((rows, LANES), 1) == e
-        gates = gate[d].reshape(rows, LANES).astype(jnp.float32)
-        gate_float = jnp.sum(jnp.where(own_col, gates, 0.0), axis=1, keepdims=True)
+        own_row = jnp.where(iota((PACKED, LANES), 0) == e, 1.0, 0.0).astype(jnp.bfloat16)
+        gate_float = jnp.concatenate(
+            [
+                lax.dot_general(
+                    gate[d, slot, :, :cap], own_row, CONTRACT_ROWS, preferred_element_type=jnp.float32
+                )
+                for slot in range(EPG)
+            ],
+            axis=0,
+        )[:, :1]
         sigma = jax.nn.sigmoid(pre_gate)
         swish = pre_gate * sigma
         hidden = swish * pre_up
@@ -435,7 +469,6 @@
         wt[at, :] = (gate_float * hidden).astype(jnp.bfloat16)
         gate_out = jnp.where(own_col, gate_part, 0.0).astype(jnp.bfloat16)
 
-        packed_width = part_g.shape[3]
         blocks = gate_out.reshape(EPG, cap, LANES)
         if packed_width > cap:
             filler = jnp.zeros((EPG, packed_width - cap, LANES), jnp.bfloat16)
@@ -516,19 +549,24 @@
         rows_at, gates_at, at = (ret, ret_g, g) if d == 0 else (done, done_g, d)
         for copy in s["l0"]:
             copy.wait_recv()
+        there = (partner(g, d, groups, 1), e, y)
+        s["z"] = []
+
+        def home(*pieces):
+            if d:
+                s["z"] += [copies.start(src, dst, there) for src, dst in pieces]
+
+        head, tail = pl.ds(0, wide0), pl.ds(wide0, wide1)
         rows_at[at, :, :wide0] = add(s2_a[d, y], *[rl_a[d, i] for i in range(lanes - 1)])
+        home((done.at[d, :, head], ret.at[g, :, head]))
         for copy in s["lg"]:
             copy.wait_recv()
         gates_at[at] = add(s2_g[d], *[rl_g[d, i] for i in range(lanes - 1)])
         if wide1:
             s["x1"].wait_recv()
             rows_at[at, :, wide0:] = add(s2_b[d, 0], rx_b[d])
-        if d:
-            there = (partner(g, d, groups, 1), e, y)
-            s["z"] = [
-                copies.start(done.at[d], ret.at[g], there),
-                copies.start(done_g.at[d], ret_g.at[g], there),
-            ]
+            home((done.at[d, :, tail], ret.at[g, :, tail]))
+        home((done_g.at[d], ret_g.at[g]))
 
     tile = min(2 * LANES, piece)
     per = piece // tile
@@ -564,7 +602,7 @@
 
     phases = {
         "own": own, "arrive_t": arrive_t, "arrive_c": arrive_c, "relay_t": relay_t,
-        "relay_c": relay_c, "inside_t": inside_t, "inside_z": inside_z, "inside_c": inside_c, "compute": compute,
+        "relay_c": relay_c, "inside_t": inside_t, "inside_z": inside_z, "inside_c": inside_c, "compute": compute, "compute_t": compute_t,
         "sum_cores": sum_cores, "middle_sum": middle_sum, "last_sum": last_sum,
         "weights": weights, "next_t": next_t, "next_c": next_c, "rest_t": rest_t, "rest_c": rest_c,
     }
@@ -627,15 +665,16 @@
             buffer(groups, cap, token_count),
             buffer(groups, cap, piece),
             buffer(groups, cap, piece),
-            buffer(groups, cap, LANES),
+            buffer(groups, PACKED, packed),
             buffer(2, lanes, cap, piece),
             buffer(2, lanes, cap, piece),
             buffer(lanes, groups, EPG, cap, piece),
             buffer(lanes, groups, EPG, cap, piece),
-            buffer(groups, EPG, cap, LANES),
+            buffer(groups, EPG, PACKED, packed),
             buffer(feature_count, hidden_count),
             buffer(feature_count, hidden_count),
             buffer(hidden_count, feature_count),
+            pltpu.VMEM((2, rows, hidden_count), jnp.float32),
             buffer(groups * rows, hidden_count),
             buffer(groups * rows, hidden_count),
             buffer(groups * rows, hidden_count),
@@ -677,14 +716,16 @@
     weight, weights_t, local_t, gate_grad, token_grad, first, second, third,
     group_out, expert_out, token_out, first_out, second_out, third_out, sem,
 ):
+    parts = [
+        (src.at[pl.ds(i * src.shape[0] // PARTS, src.shape[0] // PARTS)],
+         dst.at[pl.ds(i * src.shape[0] // PARTS, src.shape[0] // PARTS)])
+        for i in range(PARTS)
+        for src, dst in (
+            (first, first_out), (second, second_out), (third, third_out), (token_grad, token_out)
+        )
+    ]
     moves = [
-        pltpu.make_async_copy(src, dst, sem.at[i])
-        for i, (src, dst) in enumerate(
-            (
-                (first, first_out), (second, second_out), (third, third_out),
-                (token_grad, token_out),
-            )
-        )
+        pltpu.make_async_copy(src, dst, sem.at[i]) for i, (src, dst) in enumerate(parts)
     ]
     for move in moves:
         move.start()
@@ -714,7 +755,7 @@
         ),
         in_specs=[vmem] * 8,
         out_specs=(vmem,) * 2 + (hbm,) * 4,
-        scratch_shapes=[pltpu.SemaphoreType.DMA((4,))],
+        scratch_shapes=[pltpu.SemaphoreType.DMA((4 * PARTS,))],
         compiler_params=pltpu.CompilerParams(vmem_limit_bytes=FINISH_LIMIT),
         name="write_results",
     )(weight, weights_t, local_t, gate_grad, token_grad, first, second, third)

time: 62 us -> 59.6 us (0.961)
  Pallas kernels: 61.2 us -> 58.7 us
    pallas_call x1, Pallas kernels: 57.8 us -> 55.2 us  [route(): pl.pallas_call(functools.partial(kernel, groups, lanes, cap, wide0, wide1...]
where the time goes in v4:
time: 59.6 us; the launch traced here: 59.4 us
  Pallas kernels  58.7 us (98%)
  between operations  0.69 us (1%)
    pallas_call x1, Pallas kernels, route(): pl.pallas_call(functools.partial(kernel, groups, lanes, cap, wide0, wide1...  55.2 us
    pallas_call x1, Pallas kernels, finish(): pl.pallas_call(finish_kernel, out_shape=(like(weight), like(weights_t), l...  3.5 us

profile of v4, /device:TPU:0, one launch (start us, length us, event | category | flops | bytes accessed | tf_op | source)
XLA Modules:
  0.0 59.4 jit_solution(8899382333932896810)
XLA Ops:
  0.6 0.0 copy-start
  0.6 0.0 copy-start.1
  0.7 0.0 copy-start.2
  0.7 55.2 %routed_backward.1 = (f32[128,1024]{1,0:T(8,128)S(1)}, f32[16,128]{1,0:T(8,128)S(1)}, f32[2048,256]{1,0:T(8,128)S(1)}, f32[2048,256]{1,0:T(8,128)S(1)}, f32[256,2048]{1,0:T(8,128)S(1)}) custom-call(s32[1,128]{1,0:T(1,128)} %bitcast.21, f32[1,128]{1,0:T(1,128)} %bitcast.16, f32[2,128]{1,0:T(2,128)} %bitcast.12, s32[2,128]{1,0:T(2,128)} %bitcast.14, ...), custom_call_target="tpu_custom_call" | custom-call | tf_op jit(solution)/shard_map/routed_backward/pallas_call | solution.py:647
  55.9 0.0 copy-done
  55.9 0.0 copy-done.1
  55.9 0.0 copy-done.2
  55.9 3.5 %write_results.1 = (f32[1,128]{1,0:T(1,128)}, f32[2,128]{1,0:T(2,128)}, f32[128,1024]{1,0:T(8,128)}, f32[2048,256]{1,0:T(8,128)}, f32[2048,256]{1,0:T(8,128)}, /*index=5*/f32[256,2048]{1,0:T(8,128)}) custom-call(f32[1,128]{1,0:T(1,128)S(1)} %bitcast.17, f32[2,128]{1,0:T(2,128)S(1)} %bitcast.13, s32[2,128]{1,0:T(2,128)S(1)} %bitcast.15, ...), custom_call_target="tpu_custom_call" | custom-call | tf_op jit(solution)/shard_map/write_results/pallas_call | solution.py:751
Async XLA Ops:
  0.6 55.2 %copy-start = (f32[128,2]{0,1:T(2,128)S(1)}, f32[128,2]{0,1:T(2,128)}, u32[]{:S(2)}) copy-start(f32[128,2]{0,1:T(2,128)} %param.12) | copy-start | bytes 3076
  0.6 55.2 %copy-start.1 = (s32[128,2]{0,1:T(2,128)S(1)}, s32[128,2]{0,1:T(2,128)}, u32[]{:S(2)}) copy-start(s32[128,2]{0,1:T(2,128)} %param.14) | copy-start | bytes 3076
  0.7 55.2 %copy-start.2 = (f32[128]{0:T(128)S(1)}, f32[128]{0:T(128)}, u32[]{:S(2)}) copy-start(f32[128]{0:T(128)} %param.11) | copy-start | bytes 1540

commit v5 on v4

--- a/solution.py
+++ b/solution.py
@@ -10,8 +10,8 @@
 EPG = 4
 LANES = 128
 PACKED = 16
-SENDS = 32
-PARTS = 4
+SENDS = 20
+PARTS = 1
 VMEM_LIMIT = 36 * 1024 * 1024
 FINISH_LIMIT = 16 * 1024 * 1024
 

time: 59.6 us -> 59.4 us (level)
  no operation moved by 1% of the time
where the time goes in v5:
time: 59.4 us; the launch traced here: 59.2 us
  Pallas kernels  58.5 us (98%)
  between operations  0.69 us (1%)
    pallas_call x1, Pallas kernels, route(): pl.pallas_call(functools.partial(kernel, groups, lanes, cap, wide0, wide1...  55.1 us
    pallas_call x1, Pallas kernels, finish(): pl.pallas_call(finish_kernel, out_shape=(like(weight), like(weights_t), l...  3.41 us

profile of v5, /device:TPU:0, one launch (start us, length us, event | category | flops | bytes accessed | tf_op | source)
XLA Modules:
  0.0 59.2 jit_solution(1670537925303172752)
XLA Ops:
  0.6 0.0 copy-start
  0.6 0.0 copy-start.1
  0.7 0.0 copy-start.2
  0.7 55.1 %routed_backward.1 = (f32[128,1024]{1,0:T(8,128)S(1)}, f32[16,128]{1,0:T(8,128)S(1)}, f32[2048,256]{1,0:T(8,128)S(1)}, f32[2048,256]{1,0:T(8,128)S(1)}, f32[256,2048]{1,0:T(8,128)S(1)}) custom-call(s32[1,128]{1,0:T(1,128)} %bitcast.21, f32[1,128]{1,0:T(1,128)} %bitcast.16, f32[2,128]{1,0:T(2,128)} %bitcast.12, s32[2,128]{1,0:T(2,128)} %bitcast.14, ...), custom_call_target="tpu_custom_call" | custom-call | tf_op jit(solution)/shard_map/routed_backward/pallas_call | solution.py:647
  55.8 0.0 copy-done
  55.8 0.0 copy-done.1
  55.8 0.0 copy-done.2
  55.8 3.4 %write_results.1 = (f32[1,128]{1,0:T(1,128)}, f32[2,128]{1,0:T(2,128)}, f32[128,1024]{1,0:T(8,128)}, f32[2048,256]{1,0:T(8,128)}, f32[2048,256]{1,0:T(8,128)}, /*index=5*/f32[256,2048]{1,0:T(8,128)}) custom-call(f32[1,128]{1,0:T(1,128)S(1)} %bitcast.17, f32[2,128]{1,0:T(2,128)S(1)} %bitcast.13, s32[2,128]{1,0:T(2,128)S(1)} %bitcast.15, ...), custom_call_target="tpu_custom_call" | custom-call | tf_op jit(solution)/shard_map/write_results/pallas_call | solution.py:751
Async XLA Ops:
  0.6 55.1 %copy-start = (f32[128,2]{0,1:T(2,128)S(1)}, f32[128,2]{0,1:T(2,128)}, u32[]{:S(2)}) copy-start(f32[128,2]{0,1:T(2,128)} %param.12) | copy-start | bytes 3076
  0.6 55.1 %copy-start.1 = (s32[128,2]{0,1:T(2,128)S(1)}, s32[128,2]{0,1:T(2,128)}, u32[]{:S(2)}) copy-start(s32[128,2]{0,1:T(2,128)} %param.14) | copy-start | bytes 3076
  0.7 55.1 %copy-start.2 = (f32[128]{0:T(128)S(1)}, f32[128]{0:T(128)}, u32[]{:S(2)}) copy-start(f32[128]{0:T(128)} %param.11) | copy-start | bytes 1540
